TPU v7x, 128 devices: a whole 4x4x4 slice. The times are simulated.
128 devices in a mesh: kv: 16 (over z, y), tp: 8 (over x, core).
Axes of the slice: x: 4, y: 4, z: 4, core: 2. Of those that a mesh axis runs over, the one named last changes fastest.
Arguments:
- activations: bfloat16 [128, 4096], P(None, ('kv', 'tp')), may hold values from -60 to 60
- mixer_gain: bfloat16 [4096], P(('kv', 'tp')), may hold values from 0.099609375 to 1.8984375
- channel_gain: bfloat16 [4096], P(('kv', 'tp')), may hold values from 0.099609375 to 1.8984375
- query_weight: bfloat16 [4096, 4096], P('kv', 'tp'), may hold values from -0.09375 to 0.09375
- key_weight: bfloat16 [4096, 4096], P('kv', 'tp'), may hold values from -0.09375 to 0.09375
- value_weight: bfloat16 [4096, 8192], P('kv', 'tp'), may hold values from -0.09375 to 0.09375
- gate_weight: bfloat16 [4096, 8192], P('kv', 'tp'), may hold values from -0.09375 to 0.09375
- output_weight: bfloat16 [8192, 4096], P('tp', 'kv'), may hold values from -0.1875 to 0.1875
- up_weight: bfloat16 [4096, 16384], P('kv', 'tp'), may hold values from -0.09375 to 0.09375
- down_weight: bfloat16 [16384, 4096], P('tp', 'kv'), may hold values from -0.046875 to 0.046875
- state_in: float32 [128, 16, 256, 512], P('kv', 'tp'), may hold values from -0.5 to 0.5
Outputs:
- activations_out: bfloat16 [128, 4096], P(None, ('kv', 'tp'))
- state_out: float32 [128, 16, 256, 512], P('kv', 'tp')
All inputs are finite; a program needn't handle non-finite values.
Results may differ from a plain program's by a relative error of at most 0.022.
Values may be sent and summed in bfloat16 or wider, within the bound.
A program may use at most 64 MiB of HBM per device.

v0:
```python
import jax
import jax.numpy as jnp
from jax import lax
from jax.sharding import PartitionSpec as P

D = 4096
HEADS = 16
DK = 256
DV = 512


EPS = 1e-06


def sent_to_all(value, axis):
    size = lax.axis_size(axis)
    return lax.all_to_all(
        jnp.broadcast_to(value[None], (size, *value.shape)), axis, 0, 0, tiled=True
    )


def in_order(parts, dim):
    parts = jnp.moveaxis(parts, 0, dim)
    dims = parts.shape
    return parts.reshape(*dims[:dim], dims[dim] * dims[dim + 1], *dims[dim + 2 :])


def collect(value, axis, dim):
    parts = sent_to_all(value, axis)
    return in_order(parts, dim)


def split_up(value, dim, size):
    before, after = (value.shape[:dim], value.shape[dim + 1 :])
    return jnp.moveaxis(value.reshape(*before, size, -1, *after), dim, 0)


def sum_at_owner(value, axis, dim):
    size = lax.axis_size(axis)
    parts = lax.all_to_all(split_up(value, dim, size), axis, 0, 0, tiled=True)
    return jnp.sum(parts.astype(jnp.float32), axis=0)


def side_by_side(arrays, axis, dim, along):
    both = jnp.concatenate(arrays, axis=along)
    filled, at, gathered = (sum_at_owner(both, axis, dim), 0, [])
    for a in arrays:
        gathered.append(lax.slice_in_dim(filled, at, at + a.shape[along], axis=along))
        at += a.shape[along]
    return tuple(gathered)


def head_decays(count):
    index = jnp.arange(count, dtype=jnp.float32)
    return 1.0 - 2.0 ** (-1.0 - 6.0 * index / (count - 1))


def select_rows(values, groups):
    shaped = values.reshape((groups, -1) + values.shape[1:])
    return shaped.reshape((-1,) + values.shape[1:])


def retain(query_sum, key_sum, value_sum, gate_sum, scale_rows, old_state, rates):
    count, heads = (old_state.shape[0], old_state.shape[1])
    query = (scale_rows * query_sum).reshape(count, heads, DK)
    key = (scale_rows * key_sum * DK ** (-0.5)).reshape(count, heads, DK)
    value = (scale_rows * value_sum).reshape(count, heads, DV)
    gate = scale_rows * gate_sum
    new_state = rates[None, :, None, None] * old_state + key[:, :, :, None] * value[:, :, None, :]
    output = jnp.einsum("shd,shde->she", query, new_state, precision=lax.Precision.HIGHEST)
    output = output * lax.rsqrt(jnp.mean(output * output, axis=2, keepdims=True) + EPS)
    mixed = (jax.nn.silu(gate) * output.reshape(count, heads * DV)).astype(jnp.bfloat16)
    return (new_state, mixed)


def per_device(
    activations,
    mixer_gain,
    channel_gain,
    query_weight,
    key_weight,
    value_weight,
    gate_weight,
    output_weight,
    up_weight,
    down_weight,
    state_in,
):
    groups = lax.axis_size("kv")
    heads_dev = state_in.shape[1]
    rates = lax.dynamic_slice_in_dim(
        head_decays(HEADS), lax.axis_index("tp") * heads_dev, heads_dev, 0
    )
    stream = activations.astype(jnp.float32)
    squares = jnp.sum(stream * stream, axis=1, keepdims=True)
    normed = (stream * mixer_gain.astype(jnp.float32)).astype(jnp.bfloat16)
    block, square_cols = (
        collect(normed, "tp", 1),
        collect(squares.astype(jnp.bfloat16), "tp", 1).astype(squares.dtype),
    )
    block_squares = jnp.sum(square_cols, axis=1, keepdims=True)
    rows = select_rows(block, groups)
    query_term = jnp.dot(rows, query_weight, preferred_element_type=jnp.float32)
    key_term = jnp.dot(rows, key_weight, preferred_element_type=jnp.float32)
    value_term = jnp.dot(rows, value_weight, preferred_element_type=jnp.float32)
    gate_term = jnp.dot(rows, gate_weight, preferred_element_type=jnp.float32)
    query_sum, key_sum, value_sum, gate_sum, piece_totals = side_by_side(
        (
            query_term.astype(jnp.bfloat16),
            key_term.astype(jnp.bfloat16),
            value_term.astype(jnp.bfloat16),
            gate_term.astype(jnp.bfloat16),
            select_rows(block_squares, groups).astype(jnp.bfloat16),
        ),
        "kv",
        0,
        1,
    )
    scale_rows = lax.rsqrt(piece_totals / D + EPS)
    new_state, mixed = retain(query_sum, key_sum, value_sum, gate_sum, scale_rows, state_in, rates)
    out_terms = jnp.dot(collect(mixed, "kv", 0), output_weight, preferred_element_type=jnp.float32)
    attention = sum_at_owner(out_terms.astype(jnp.bfloat16), "tp", 1)
    middle = (stream + attention).astype(jnp.bfloat16)
    middle = lax.optimization_barrier(middle).astype(jnp.float32)
    middle_squares = jnp.sum(middle * middle, axis=1, keepdims=True)
    channel_normed = (middle * channel_gain.astype(jnp.float32)).astype(jnp.bfloat16)
    channel_block, channel_cols = (
        collect(channel_normed, "tp", 1),
        collect(middle_squares.astype(jnp.bfloat16), "tp", 1).astype(middle_squares.dtype),
    )
    up_sum, own_channel = side_by_side(
        (
            jnp.dot(channel_block, up_weight, preferred_element_type=jnp.float32).astype(
                jnp.bfloat16
            ),
            jnp.sum(channel_cols, axis=1, keepdims=True).astype(jnp.bfloat16),
        ),
        "kv",
        0,
        1,
    )
    lifted = lax.rsqrt(own_channel / D + EPS) * up_sum
    hidden = jnp.square(jax.nn.relu(lifted)).astype(jnp.bfloat16)
    down_terms = jnp.dot(collect(hidden, "kv", 0), down_weight, preferred_element_type=jnp.float32)
    lowered = sum_at_owner(down_terms.astype(jnp.bfloat16), "tp", 1)
    return ((middle + lowered).astype(jnp.bfloat16), new_state)


def solution(mesh):
    return jax.shard_map(
        per_device,
        mesh=mesh,
        in_specs=(
            P(None, ("kv", "tp")),
            P(("kv", "tp")),
            P(("kv", "tp")),
            P("kv", "tp"),
            P("kv", "tp"),
            P("kv", "tp"),
            P("kv", "tp"),
            P("tp", "kv"),
            P("kv", "tp"),
            P("tp", "kv"),
            P("kv", "tp", None, None),
        ),
        out_specs=(P(None, ("kv", "tp")), P("kv", "tp", None, None)),
        check_vma=False,
    )
```

profile of v0, /device:TPU:1, one launch (start us, length us, event | category | flops | bytes accessed | tf_op | source)
XLA Modules:
  0.0 141.7 jit_solution(3297570347268671122)
XLA Ops:
  0.6 0.7 convert_element_type.112
  1.4 0.8 fusion.16
  2.2 10.2 %all_to_all.50 = bf16[8,128,1]{1,2,0:T(2,128)(2,1)S(1)} all-to-all(bf16[8,128,1]{1,2,0:T(2,128)(2,1)S(1)} %broadcast_in_dim.13), channel_id=1, replica_groups=mesh['kv'=16,'tp'=8] {'tp'}, dimensions={0} | all-to-all | bytes 4096 | tf_op jit(solution)/shard_map/all_to_all | solution.py:17
  13.0 3.9 %all-to-all-start = ((bf16[8,128,32]{1,2,0:T(8,128)(2,1)}), bf16[8,128,32]{1,2,0:T(8,128)(2,1)S(1)}, u32[]{:S(2)}, u32[]{:S(2)}) async-start(bf16[8,128,32]{1,2,0:T(8,128)(2,1)} %broadcast_in_dim.12), calls=%async_computation | async-start | bytes 131072 | tf_op jit(solution)/shard_map/all_to_all | solution.py:17
  17.2 4.6 %all-to-all-done = bf16[8,128,32]{1,2,0:T(8,128)(2,1)S(1)} async-done(((bf16[8,128,32]{1,2,0:T(8,128)(2,1)}), bf16[8,128,32]{1,2,0:T(8,128)(2,1)S(1)}, u32[]{:S(2)}, u32[]{:S(2)}) %all-to-all-start) | async-done | bytes 65568 | tf_op jit(solution)/shard_map/all_to_all | solution.py:17
  21.8 1.8 %fusion.6 = bf16[16,8,3073]{2,1,0:T(8,128)(2,1)} fusion(bf16[128,256]{0,1:T(8,128)(2,1)S(1)} %bitcast.60, bf16[256,512]{1,0:T(8,128)(2,1)} %param.14), kind=kOutput, calls=%fused_computation.13 | convolution fusion | flops 33619968 | bytes 458752 | tf_op jit(solution)/shard_map/dot_general | solution.py:103
  23.6 1.8 %fusion.8 = bf16[16,8,3073]{2,1,0:T(8,128)(2,1)} fusion(bf16[16,8,3073]{2,1,0:T(8,128)(2,1)} %fusion.6, bf16[128,256]{0,1:T(8,128)(2,1)S(1)} %bitcast.61, bf16[256,512]{1,0:T(8,128)(2,1)} %param.15), kind=kOutput, calls=%fused_computation.15 | convolution fusion | flops 33619968 | bytes 458752 | tf_op jit(solution)/shard_map/dot_general | solution.py:104
  25.4 2.0 %fusion.2 = bf16[16,8,3073]{2,1,0:T(8,128)(2,1)} fusion(bf16[16,8,3073]{2,1,0:T(8,128)(2,1)} %fusion.8, bf16[128,256]{0,1:T(8,128)(2,1)S(1)} %bitcast.62, bf16[256,1024]{1,0:T(8,128)(2,1)} %param.16), kind=kOutput, calls=%fused_computation.7 | convolution fusion | flops 67239936 | bytes 851968 | tf_op jit(solution)/shard_map/dot_general | solution.py:105
  27.4 2.0 %fusion.4 = bf16[16,8,3073]{2,1,0:T(8,128)(2,1)} fusion(bf16[16,8,3073]{2,1,0:T(8,128)(2,1)} %fusion.2, bf16[128,256]{0,1:T(8,128)(2,1)S(1)} %bitcast.63, bf16[256,1024]{1,0:T(8,128)(2,1)} %param.17), kind=kOutput, calls=%fused_computation.9 | convolution fusion | flops 67239936 | bytes 851968 | tf_op jit(solution)/shard_map/dot_general | solution.py:106
  30.1 7.8 %all-to-all-start.2 = ((bf16[16,8,3073]{2,1,0:T(8,128)(2,1)}), bf16[16,8,3073]{2,1,0:T(8,128)(2,1)S(1)}, u32[]{:S(2)}, u32[]{:S(2)}) async-start(bf16[16,8,3073]{2,1,0:T(8,128)(2,1)} %constant_dynamic-update-slice_fusion), calls=%async_computation.2 | async-start | bytes 1638400 | tf_op jit(solution)/shard_map/all_to_all | solution.py:40
  37.9 13.4 %all-to-all-done.2 = bf16[16,8,3073]{2,1,0:T(8,128)(2,1)S(1)} async-done(((bf16[16,8,3073]{2,1,0:T(8,128)(2,1)}), bf16[16,8,3073]{2,1,0:T(8,128)(2,1)S(1)}, u32[]{:S(2)}, u32[]{:S(2)}) %all-to-all-start.2) | async-done | bytes 786720 | tf_op jit(solution)/shard_map/all_to_all | solution.py:40
  51.8 4.1 %multiply_add_fusion = f32[8,2,256,512]{3,2,1,0:T(8,128)S(1)} fusion(f32[8,2,256,512]{3,2,1,0:T(8,128)} %param.21, f32[8,2,512]{2,1,0:T(2,128)S(1)} %copy.37, f32[8,2,256]{2,1,0:T(2,128)S(1)} %copy.36, f32[2]{0:T(128)S(1)} %dynamic_slice.3), kind=kLoop, calls=%fused_computation | loop fusion | flops 6291456 | bytes 16826376 | tf_op jit(solution)/shard_map/add | solution.py:69
  55.9 3.4 %copy-done.1 = f32[8,2,256,512]{3,2,1,0:T(8,128)} copy-done((f32[8,2,256,512]{3,2,1,0:T(8,128)}, f32[8,2,256,512]{3,2,1,0:T(8,128)S(1)}, u32[]{:S(2)}) %copy-start.1) | copy-done | bytes 8388632
  59.3 4.1 %fusion.22 = f32[8,2,1,512]{3,2,1,0:T(1,128)S(1)} fusion(f32[8,2,256,512]{3,2,1,0:T(8,128)S(1)} %multiply_add_fusion, f32[8,2,256,1]{2,0,1,3:T(8,128)S(1)} %bitcast.68), kind=kOutput, calls=%fused_computation.49 | convolution fusion | flops 25165824 | bytes 8437760 | tf_op jit(solution)/shard_map/shd,shde->she/dot_general | solution.py:70
  63.6 11.4 %all_to_all.51 = bf16[16,8,1024]{2,1,0:T(8,128)(2,1)S(1)} all-to-all(bf16[16,8,1024]{2,1,0:T(8,128)(2,1)S(1)} %broadcast_in_dim.14), channel_id=1, replica_groups=mesh['kv'=16,'tp'=8] {'kv'}, dimensions={0} | all-to-all | bytes 524288 | tf_op jit(solution)/shard_map/all_to_all | solution.py:17
  75.2 0.7 copy.38
  75.9 5.6 %all-to-all-start.4 = ((bf16[8,128,32]{1,2,0:T(8,128)(2,1)}), bf16[8,128,32]{1,2,0:T(8,128)(2,1)S(1)}, u32[]{:S(2)}, u32[]{:S(2)}) async-start(bf16[8,128,32]{1,2,0:T(8,128)(2,1)} %bitcast.15), calls=%async_computation.4 | async-start | bytes 131072 | tf_op jit(solution)/shard_map/all_to_all | solution.py:40
  81.5 4.9 %all-to-all-done.4 = bf16[8,128,32]{1,2,0:T(8,128)(2,1)S(1)} async-done(((bf16[8,128,32]{1,2,0:T(8,128)(2,1)}), bf16[8,128,32]{1,2,0:T(8,128)(2,1)S(1)}, u32[]{:S(2)}, u32[]{:S(2)}) %all-to-all-start.4) | async-done | bytes 65568 | tf_op jit(solution)/shard_map/all_to_all | solution.py:40
  86.5 7.7 %all_to_all.52 = bf16[8,128,1]{1,2,0:T(2,128)(2,1)S(1)} all-to-all(bf16[8,128,1]{1,2,0:T(2,128)(2,1)S(1)} %broadcast_in_dim.16), channel_id=1, replica_groups=mesh['kv'=16,'tp'=8] {'tp'}, dimensions={0} | all-to-all | bytes 4096 | tf_op jit(solution)/shard_map/all_to_all | solution.py:17
  94.8 3.9 %all-to-all-start.5 = ((bf16[8,128,32]{1,2,0:T(8,128)(2,1)}), bf16[8,128,32]{1,2,0:T(8,128)(2,1)S(1)}, u32[]{:S(2)}, u32[]{:S(2)}) async-start(bf16[8,128,32]{1,2,0:T(8,128)(2,1)} %broadcast_in_dim.15), calls=%async_computation.5 | async-start | bytes 131072 | tf_op jit(solution)/shard_map/all_to_all | solution.py:17
  99.1 4.6 %all-to-all-done.5 = bf16[8,128,32]{1,2,0:T(8,128)(2,1)S(1)} async-done(((bf16[8,128,32]{1,2,0:T(8,128)(2,1)}), bf16[8,128,32]{1,2,0:T(8,128)(2,1)S(1)}, u32[]{:S(2)}, u32[]{:S(2)}) %all-to-all-start.5) | async-done | bytes 65568 | tf_op jit(solution)/shard_map/all_to_all | solution.py:17
  104.1 13.7 %all_to_all.53 = bf16[16,8,2049]{2,1,0:T(8,128)(2,1)S(1)} all-to-all(bf16[16,8,2049]{2,1,0:T(8,128)(2,1)S(1)} %pad_maximum_fusion), channel_id=1, replica_groups=mesh['kv'=16,'tp'=8] {'kv'}, dimensions={0} | all-to-all | bytes 1049088 | tf_op jit(solution)/shard_map/all_to_all | solution.py:40
  118.1 12.2 %all_to_all.54 = bf16[16,8,2048]{2,1,0:T(8,128)(2,1)S(1)} all-to-all(bf16[16,8,2048]{2,1,0:T(8,128)(2,1)S(1)} %broadcast_in_dim.17), channel_id=1, replica_groups=mesh['kv'=16,'tp'=8] {'kv'}, dimensions={0} | all-to-all | bytes 1048576 | tf_op jit(solution)/shard_map/all_to_all | solution.py:17
  130.8 10.3 %all_to_all.55 = bf16[8,128,32]{1,2,0:T(8,128)(2,1)S(1)} all-to-all(bf16[8,128,32]{1,2,0:T(8,128)(2,1)S(1)} %bitcast.65), channel_id=1, replica_groups=mesh['kv'=16,'tp'=8] {'tp'}, dimensions={0} | all-to-all | bytes 131072 | tf_op jit(solution)/shard_map/all_to_all | solution.py:40
  (48 shorter events, 5.3 us)
Async XLA Ops:
  0.6 103.0 %copy-start = (bf16[256,2048]{1,0:T(8,128)(2,1)S(1)}, bf16[256,2048]{1,0:T(8,128)(2,1)}, u32[]{:S(2)}) copy-start(bf16[256,2048]{1,0:T(8,128)(2,1)} %param.19) | copy-start | bytes 3145732
  13.0 8.8 %all-to-all-start = ((bf16[8,128,32]{1,2,0:T(8,128)(2,1)}), bf16[8,128,32]{1,2,0:T(8,128)(2,1)S(1)}, u32[]{:S(2)}, u32[]{:S(2)}) async-start(bf16[8,128,32]{1,2,0:T(8,128)(2,1)} %broadcast_in_dim.12), calls=%async_computation | async-start | bytes 131072 | tf_op jit(solution)/shard_map/all_to_all | solution.py:17
  30.1 21.3 %all-to-all-start.2 = ((bf16[16,8,3073]{2,1,0:T(8,128)(2,1)}), bf16[16,8,3073]{2,1,0:T(8,128)(2,1)S(1)}, u32[]{:S(2)}, u32[]{:S(2)}) async-start(bf16[16,8,3073]{2,1,0:T(8,128)(2,1)} %constant_dynamic-update-slice_fusion), calls=%async_computation.2 | async-start | bytes 1638400 | tf_op jit(solution)/shard_map/all_to_all | solution.py:40
  55.9 3.4 %copy-start.1 = (f32[8,2,256,512]{3,2,1,0:T(8,128)}, f32[8,2,256,512]{3,2,1,0:T(8,128)S(1)}, u32[]{:S(2)}) copy-start(f32[8,2,256,512]{3,2,1,0:T(8,128)S(1)} %multiply_add_fusion) | copy-start | bytes 25165828
  55.9 19.1 %copy-start.3 = (bf16[1024,256]{1,0:T(8,128)(2,1)S(1)}, bf16[1024,256]{1,0:T(8,128)(2,1)}, u32[]{:S(2)}) copy-start(bf16[1024,256]{1,0:T(8,128)(2,1)} %param.18) | copy-start | bytes 1572868
  55.9 25.6 %copy-start.5 = (bf16[32]{0:T(256)(128)(2,1)S(1)}, bf16[32]{0:T(256)(128)(2,1)}, u32[]{:S(2)}) copy-start(bf16[32]{0:T(256)(128)(2,1)} %param.13) | copy-start | bytes 196
  55.9 30.5 %copy-start.4 = (bf16[128,32]{0,1:T(8,128)(2,1)S(1)}, bf16[128,32]{0,1:T(8,128)(2,1)}, u32[]{:S(2)}) copy-start(bf16[128,32]{0,1:T(8,128)(2,1)} %param.11) | copy-start | bytes 24580
  59.3 71.1 %copy-start.2 = (bf16[2048,256]{1,0:T(8,128)(2,1)S(1)}, bf16[2048,256]{1,0:T(8,128)(2,1)}, u32[]{:S(2)}) copy-start(bf16[2048,256]{1,0:T(8,128)(2,1)} %param.20) | copy-start | bytes 3145732
  75.9 10.4 %all-to-all-start.4 = ((bf16[8,128,32]{1,2,0:T(8,128)(2,1)}), bf16[8,128,32]{1,2,0:T(8,128)(2,1)S(1)}, u32[]{:S(2)}, u32[]{:S(2)}) async-start(bf16[8,128,32]{1,2,0:T(8,128)(2,1)} %bitcast.15), calls=%async_computation.4 | async-start | bytes 131072 | tf_op jit(solution)/shard_map/all_to_all | solution.py:40
  94.8 8.8 %all-to-all-start.5 = ((bf16[8,128,32]{1,2,0:T(8,128)(2,1)}), bf16[8,128,32]{1,2,0:T(8,128)(2,1)S(1)}, u32[]{:S(2)}, u32[]{:S(2)}) async-start(bf16[8,128,32]{1,2,0:T(8,128)(2,1)} %broadcast_in_dim.15), calls=%async_computation.5 | async-start | bytes 131072 | tf_op jit(solution)/shard_map/all_to_all | solution.py:17
where the time goes:
time: 143 us; the launch traced here: 142 us
  blocking collectives  65.5 us (46%)
  waiting for transfers between devices  27.5 us (19%)
  starting transfers between devices  21.2 us (15%)
  matrix products  12.6 us (9%)
  other arithmetic  7.36 us (5%)
  local copies, waits for them, and re-layouts  6.76 us (5%)
    all_to_all x4, blocking collectives, sent_to_all(): lax.all_to_all(jnp.broadcast_to(value[None], (size, *value.shape)), axis,...  41.5 us
    all_to_all x2, blocking collectives, sum_at_owner(): parts = lax.all_to_all(split_up(value, dim, size), axis, 0, 0, tiled=True)  24 us
    all_to_all x2, waiting for transfers between devices, sum_at_owner(): parts = lax.all_to_all(split_up(value, dim, size), axis, 0, 0, tiled=True)  18.2 us
    all_to_all x2, starting transfers between devices, sum_at_owner(): parts = lax.all_to_all(split_up(value, dim, size), axis, 0, 0, tiled=True)  13.3 us
    all_to_all x2, waiting for transfers between devices, sent_to_all(): lax.all_to_all(jnp.broadcast_to(value[None], (size, *value.shape)), axis,...  9.22 us
    all_to_all x2, starting transfers between devices, sent_to_all(): lax.all_to_all(jnp.broadcast_to(value[None], (size, *value.shape)), axis,...  7.89 us
    add x1, other arithmetic, retain(): rates[None, :, None, None] * old_state  4.08 us
    dot_general x1, matrix products, retain(): jnp.einsum('shd,shde->she', query, new_state, precision=lax.Precision.HIG...  4.05 us
  transfers between devices with their start and end apart: 4, of which 4 were waited for; matrix products, arithmetic and copies ran while one was open for 0% of the time, Pallas kernels for 0%

commit v1 on v0

v1 whole, which is shorter than its diff:
```python
import functools

import jax
import jax.numpy as jnp
from jax import lax
from jax.experimental import pallas as pl
from jax.experimental.pallas import tpu as pltpu
from jax.sharding import PartitionSpec as P

D = 4096
HEADS = 16
DK = 256
DV = 512
EPS = 1e-06
KV = 16
TP = 8
ROWS = 8
HPD = 2
F32 = jnp.float32
BF16 = jnp.bfloat16
MESH = pl.DeviceIdType.MESH


def start_all(axis, n, me, source, dest, send, recv):
    for d in range(1, n):
        peer = lax.rem(me + d, n)
        pltpu.make_async_remote_copy(
            src_ref=source(peer),
            dst_ref=dest.at[me],
            send_sem=send.at[d],
            recv_sem=recv.at[d],
            device_id={axis: peer},
            device_id_type=MESH,
        ).start()


def wait_all(axis, n, me, source, dest, send, recv, which):
    for d in range(1, n):
        peer = lax.rem(me + n - d, n) if which == "recv" else lax.rem(me + d, n)
        copy = pltpu.make_async_remote_copy(
            src_ref=source(peer),
            dst_ref=dest.at[peer],
            send_sem=send.at[d],
            recv_sem=recv.at[d],
            device_id={axis: peer},
            device_id_type=MESH,
        )
        if which == "recv":
            copy.wait_recv()
        else:
            copy.wait_send()


def total(ref, n):
    acc = ref[0].astype(F32)
    for j in range(1, n):
        acc = acc + ref[j].astype(F32)
    return acc


def kernel(
    x_ref, gains_ref, wq_ref, wk_ref, wv_ref, wg_ref, wo_ref, wu_ref, wd_ref, state_ref,
    out_ref, state_out_ref,
    wq, wk, wv, wg, wo, wu, wd, st,
    s1, r1, sa, ra, sv, rv, sg, rg, r4, s5, r5, r6,
    sb0, rb0, sb1, rb1, s7, r7, s8, r8,
    xrows, qt, kt, ret, midt,
    lsem, ss1, rs1, ssa, rsa, ssv, rsv, ssg, rsg, ss4, rs4, ss5, rs5, ss6, rs6,
    ssb0, rsb0, ssb1, rsb1, ss7, rs7, ss8, rs8,
):
    kv = lax.axis_index("kv")
    tp = lax.axis_index("tp")
    barrier = pltpu.get_barrier_semaphore()
    for d in range(1, TP):
        pl.semaphore_signal(barrier, inc=1, device_id={"tp": lax.rem(tp + d, TP)}, device_id_type=MESH)
    for d in range(1, KV):
        pl.semaphore_signal(barrier, inc=1, device_id={"kv": lax.rem(kv + d, KV)}, device_id_type=MESH)
    local = [
        pltpu.make_async_copy(a, b, lsem.at[i])
        for i, (a, b) in enumerate(
            ((wq_ref, wq), (wk_ref, wk), (wv_ref, wv), (wg_ref, wg), (state_ref, st),
             (wo_ref, wo), (wu_ref, wu), (wd_ref, wd))
        )
    ]
    for c in local:
        c.start()

    s1[0:32, :] = jnp.transpose(x_ref[...].astype(F32)).astype(BF16)
    lane = lax.broadcasted_iota(jnp.int32, (16, 128), 1)
    s1[32:48, :] = jnp.where(lane // 32 == lax.rem(tp, 4), gains_ref[...].astype(F32), 0.0).astype(BF16)
    r1[tp] = s1[...]
    pl.semaphore_wait(barrier, TP - 1 + KV - 1)

    one = lambda peer: s1
    start_all("tp", TP, tp, one, r1, ss1, rs1)
    wait_all("tp", TP, tp, one, r1, ss1, rs1, "recv")
    xt = jnp.concatenate([r1[j, 0:32, :].astype(F32) for j in range(TP)], axis=0)
    x = jnp.transpose(xt)
    xrows[...] = x
    halves = [sum(r1[j, 32:48, :].astype(F32) for j in range(4 * i, 4 * i + 4)) for i in range(2)]
    gains = jnp.concatenate(halves, axis=1)
    normed = (x * gains[0:1, :]).astype(BF16)
    squares = jnp.sum(x * x, axis=1, keepdims=True)

    for c in local[:2]:
        c.wait()
    sa[:, :, 0:512] = jnp.dot(normed, wq[...], preferred_element_type=F32).astype(BF16).reshape(KV, ROWS, 512)
    sa[:, :, 512:1024] = jnp.dot(normed, wk[...], preferred_element_type=F32).astype(BF16).reshape(KV, ROWS, 512)
    sa[:, :, 1024:1152] = jnp.broadcast_to(squares, (128, 128)).astype(BF16).reshape(KV, ROWS, 128)
    start_all("kv", KV, kv, lambda peer: sa.at[peer], ra, ssa, rsa)
    local[2].wait()
    sv[...] = jnp.dot(normed, wv[...], preferred_element_type=F32).astype(BF16).reshape(KV, ROWS, 1024)
    start_all("kv", KV, kv, lambda peer: sv.at[peer], rv, ssv, rsv)
    local[3].wait()
    sg[...] = jnp.dot(normed, wg[...], preferred_element_type=F32).astype(BF16).reshape(KV, ROWS, 1024)
    start_all("kv", KV, kv, lambda peer: sg.at[peer], rg, ssg, rsg)
    ra[kv] = sa[kv]
    rv[kv] = sv[kv]
    rg[kv] = sg[kv]

    wait_all("kv", KV, kv, lambda peer: sa.at[peer], ra, ssa, rsa, "recv")
    sums = total(ra, KV)
    scale = lax.rsqrt(sums[:, 1024:1025] / D + EPS)
    query = scale * sums[:, 0:512]
    key = scale * sums[:, 512:1024] * DK ** (-0.5)
    qt[...] = jnp.transpose(query)
    kt[...] = jnp.transpose(key)
    local[4].wait()
    for b in range(ROWS):
        for h in range(HPD):
            col = qt[h * DK : (h + 1) * DK, b : b + 1]
            ret[b : b + 1, h * DV : (h + 1) * DV] = jnp.sum(st[b, h] * col, axis=0, keepdims=True)
    wait_all("kv", KV, kv, lambda peer: sv.at[peer], rv, ssv, rsv, "recv")
    value = scale * total(rv, KV)
    wait_all("kv", KV, kv, lambda peer: sg.at[peer], rg, ssg, rsg, "recv")
    gate = scale * total(rg, KV)
    gate = gate * jax.nn.sigmoid(gate)
    rates = []
    for h in range(HPD):
        head = (tp * HPD + h).astype(F32)
        vec = jnp.full((1, 128), head, F32)
        rates.append((1.0 - jnp.exp2(-1.0 - 6.0 * vec / (HEADS - 1)))[:, 0:1])
        qk = jnp.sum(query[:, h * DK : (h + 1) * DK] * key[:, h * DK : (h + 1) * DK], axis=1, keepdims=True)
        cols = slice(h * DV, (h + 1) * DV)
        out = rates[h] * ret[:, cols] + qk * value[:, cols]
        out = out * lax.rsqrt(jnp.mean(out * out, axis=1, keepdims=True) + EPS)
        r4[pl.ds(kv, 1), :, cols] = (gate[:, cols] * out).astype(BF16)[None]

    own = lambda peer: r4.at[kv]
    start_all("kv", KV, kv, own, r4, ss4, rs4)
    ret[...] = value
    for b in range(ROWS):
        for h in range(HPD):
            col = kt[h * DK : (h + 1) * DK, b : b + 1]
            st[b, h] = rates[h] * st[b, h] + col * ret[b : b + 1, h * DV : (h + 1) * DV]
    state_copy = pltpu.make_async_copy(st, state_out_ref, lsem.at[8])
    state_copy.start()
    local[5].wait()
    wait_all("kv", KV, kv, own, r4, ss4, rs4, "recv")
    mixed = r4[...].astype(F32).reshape(128, HPD * DV).astype(BF16)
    terms = jnp.dot(mixed, wo[...], preferred_element_type=F32)
    s5[...] = terms.astype(BF16).reshape(TP, 16, 256)

    start_all("tp", TP, tp, lambda peer: s5.at[peer], r5, ss5, rs5)
    r5[tp] = s5[tp]
    wait_all("tp", TP, tp, lambda peer: s5.at[peer], r5, ss5, rs5, "recv")
    attention = total(r5, TP)
    r6[tp] = (xrows[pl.ds(pl.multiple_of(tp * 16, 16), 16), :] + attention).astype(BF16)
    mine = lambda peer: r6.at[tp]
    start_all("tp", TP, tp, mine, r6, ss6, rs6)
    wait_all("tp", TP, tp, mine, r6, ss6, rs6, "recv")
    middle = r6[...].astype(F32).reshape(128, 256)
    msquares = jnp.sum(middle * middle, axis=1, keepdims=True)
    cnormed = (middle * gains[1:2, :]).astype(BF16)

    local[6].wait()
    sb0[:, :, 0:1024] = jnp.dot(cnormed, wu[:, 0:1024], preferred_element_type=F32).astype(BF16).reshape(KV, ROWS, 1024)
    sb0[:, :, 1024:1152] = jnp.broadcast_to(msquares, (128, 128)).astype(BF16).reshape(KV, ROWS, 128)
    start_all("kv", KV, kv, lambda peer: sb0.at[peer], rb0, ssb0, rsb0)
    sb1[...] = jnp.dot(cnormed, wu[:, 1024:2048], preferred_element_type=F32).astype(BF16).reshape(KV, ROWS, 1024)
    start_all("kv", KV, kv, lambda peer: sb1.at[peer], rb1, ssb1, rsb1)
    rb0[kv] = sb0[kv]
    rb1[kv] = sb1[kv]
    midt[...] = jnp.transpose(middle)
    local[7].wait()
    wait_all("kv", KV, kv, lambda peer: sb0.at[peer], rb0, ssb0, rsb0, "recv")
    up0 = total(rb0, KV)
    cscale = lax.rsqrt(up0[:, 1024:1025] / D + EPS)
    hid0 = jnp.square(jnp.maximum(cscale * up0[:, 0:1024], 0.0)).astype(BF16)
    r7[pl.ds(kv, 1), :, 0:1024] = hid0[None]
    wait_all("kv", KV, kv, lambda peer: sb1.at[peer], rb1, ssb1, rsb1, "recv")
    hid1 = jnp.square(jnp.maximum(cscale * total(rb1, KV), 0.0)).astype(BF16)
    r7[pl.ds(kv, 1), :, 1024:2048] = hid1[None]

    own7 = lambda peer: r7.at[kv]
    start_all("kv", KV, kv, own7, r7, ss7, rs7)
    wait_all("kv", KV, kv, own7, r7, ss7, rs7, "recv")
    hidden = r7[...].astype(F32).reshape(128, 2048).astype(BF16)
    down = jnp.dot(hidden, wd[...], preferred_element_type=F32)
    s8[...] = jnp.transpose(down).astype(BF16).reshape(TP, 32, 128)

    start_all("tp", TP, tp, lambda peer: s8.at[peer], r8, ss8, rs8)
    r8[tp] = s8[tp]
    wait_all("tp", TP, tp, lambda peer: s8.at[peer], r8, ss8, rs8, "recv")
    lowered = total(r8, TP)
    out_ref[...] = (midt[pl.ds(pl.multiple_of(tp * 32, 32), 32), :] + lowered).astype(BF16)

    wait_all("tp", TP, tp, one, r1, ss1, rs1, "send")
    for s, r, a, b in ((sa, ra, ssa, rsa), (sv, rv, ssv, rsv), (sg, rg, ssg, rsg)):
        wait_all("kv", KV, kv, lambda peer: s.at[peer], r, a, b, "send")
    wait_all("kv", KV, kv, own, r4, ss4, rs4, "send")
    wait_all("tp", TP, tp, lambda peer: s5.at[peer], r5, ss5, rs5, "send")
    wait_all("tp", TP, tp, mine, r6, ss6, rs6, "send")
    wait_all("kv", KV, kv, lambda peer: sb0.at[peer], rb0, ssb0, rsb0, "send")
    wait_all("kv", KV, kv, lambda peer: sb1.at[peer], rb1, ssb1, rsb1, "send")
    wait_all("kv", KV, kv, own7, r7, ss7, rs7, "send")
    wait_all("tp", TP, tp, lambda peer: s8.at[peer], r8, ss8, rs8, "send")
    state_copy.wait()


def per_device(x, mixer_gain, channel_gain, wq, wk, wv, wg, wo, wu, wd, state):
    gains = jnp.pad(jnp.tile(jnp.stack([mixer_gain, channel_gain]), (1, 4)), ((0, 14), (0, 0)))
    vm = pl.BlockSpec(memory_space=pltpu.VMEM)
    hb = pl.BlockSpec(memory_space=pl.ANY)
    dma = pltpu.SemaphoreType.DMA
    v = lambda shape, dtype=BF16: pltpu.VMEM(shape, dtype)
    kvbuf = lambda n: v((KV, ROWS, n))
    scratch = [
        v((256, 512)), v((256, 512)), v((256, 1024)), v((256, 1024)),
        v((1024, 256)), v((256, 2048)), v((2048, 256)), v((ROWS, HPD, DK, DV), F32),
        v((48, 128)), v((TP, 48, 128)),
        kvbuf(1152), kvbuf(1152), kvbuf(1024), kvbuf(1024), kvbuf(1024), kvbuf(1024),
        kvbuf(1024), v((TP, 16, 256)), v((TP, 16, 256)), v((TP, 16, 256)),
        kvbuf(1152), kvbuf(1152), kvbuf(1024), kvbuf(1024),
        v((8, 128)), kvbuf(2048), v((TP, 32, 128)), v((TP, 32, 128)),
        v((128, 256), F32), v((512, ROWS), F32), v((512, ROWS), F32), v((ROWS, 1024), F32), v((256, 128), F32),
        dma((9,)),
        dma((TP,)), dma((TP,)),
        dma((KV,)), dma((KV,)), dma((KV,)), dma((KV,)), dma((KV,)), dma((KV,)),
        dma((KV,)), dma((KV,)), dma((TP,)), dma((TP,)), dma((TP,)), dma((TP,)),
        dma((KV,)), dma((KV,)), dma((KV,)), dma((KV,)), dma((KV,)), dma((KV,)),
        dma((TP,)), dma((TP,)),
    ]
    out, new_state = pl.pallas_call(
        kernel,
        name="layer",
        out_shape=(
            jax.ShapeDtypeStruct((32, 128), BF16),
            jax.ShapeDtypeStruct(state.shape, F32),
        ),
        in_specs=[vm, vm] + [hb] * 8,
        out_specs=(vm, hb),
        scratch_shapes=scratch,
        compiler_params=pltpu.CompilerParams(
            collective_id=0, has_side_effects=True, vmem_limit_bytes=40 * 2**20
        ),
    )(x, gains, wq, wk, wv, wg, wo, wu, wd, state)
    return out.T, new_state


def solution(mesh):
    return jax.shard_map(
        per_device,
        mesh=mesh,
        in_specs=(
            P(None, ("kv", "tp")),
            P(("kv", "tp")),
            P(("kv", "tp")),
            P("kv", "tp"),
            P("kv", "tp"),
            P("kv", "tp"),
            P("kv", "tp"),
            P("tp", "kv"),
            P("kv", "tp"),
            P("tp", "kv"),
            P("kv", "tp", None, None),
        ),
        out_specs=(P(None, ("kv", "tp")), P("kv", "tp", None, None)),
        check_vma=False,
    )
```

time: 143 us -> 76.6 us (0.54)
  blocking collectives: 65.5 us -> 0 us
  Pallas kernels: 0 us -> 62.5 us
  waiting for transfers between devices: 27.5 us -> 0 us
  starting transfers between devices: 21.2 us -> 0 us
  matrix products: 12.6 us -> 0 us
  other arithmetic: 7.36 us -> 0.68 us
  local copies, waits for them, and re-layouts: 6.76 us -> 12.4 us
    all_to_all x6 -> x0, blocking collectives: 65.5 us -> none  [the longest x4 41.5 us: sent_to_all(): lax.all_to_all(jnp.broadcast_to(value[None], (size, *value.shape)), axis,...]
    pallas_call x0 -> x1, Pallas kernels: none -> 62.5 us  [per_device(): pl.pallas_call(kernel, name='layer', out_shape=(jax.ShapeDtypeStruct((32,...]
    all_to_all x4 -> x0, waiting for transfers between devices: 27.5 us -> none  [the longest x2 18.2 us: sum_at_owner(): parts = lax.all_to_all(split_up(value, dim, size), axis, 0, 0, tiled=True)]
    all_to_all x4 -> x0, starting transfers between devices: 21.2 us -> none  [the longest x2 13.3 us: sum_at_owner(): parts = lax.all_to_all(split_up(value, dim, size), axis, 0, 0, tiled=True)]
    dot_general x8 -> x0, matrix products: 12.6 us -> none  [the longest x1 4.05 us: retain(): jnp.einsum('shd,shde->she', query, new_state, precision=lax.Precision.HIG...]
    unnamed x12 -> x17, local copies, waits for them, and re-layouts: 3.39 us -> 12.3 us
    add x1 -> x0, other arithmetic: 4.08 us -> none  [retain(): rates[None, :, None, None] * old_state]
    convert_element_type x7 -> x0, other arithmetic: 1.61 us -> none  [the longest x1 0.75 us: per_device(): normed = (stream * mixer_gain.astype(jnp.float32)).astype(jnp.bfloat16)]
  transfers between devices with their start and end apart: 4 -> 0, of which waited for: 4 -> 0; matrix products, arithmetic and copies ran while one was open for 0% -> 0% of each run, Pallas kernels for 0% -> 0%
where the time goes in v1:
time: 76.6 us; the launch traced here: 76.2 us
  Pallas kernels  62.5 us (82%)
  local copies, waits for them, and re-layouts  12.4 us (16%)
    pallas_call x1, Pallas kernels, per_device(): pl.pallas_call(kernel, name='layer', out_shape=(jax.ShapeDtypeStruct((32,...  62.5 us
    unnamed x17, local copies, waits for them, and re-layouts  12.3 us

profile of v1, /device:TPU:1, one launch (start us, length us, event | category | flops | bytes accessed | tf_op | source)
XLA Modules:
  0.0 76.2 jit_solution(359281622203531116)
XLA Ops:
  0.6 0.7 pad_maximum_fusion
  1.3 0.1 tile.10
  1.4 0.8 %copy.13.x_ref = bf16[128,32]{1,0:T(8,128)(2,1)S(1)} copy(bf16[128,32]{0,1:T(8,128)(2,1)} %param.11) | data formatting | bytes 16384 | tf_op args[0]
  2.2 0.0 copy-start
  2.2 1.2 %copy-done = bf16[256,2048]{1,0:T(8,128)(2,1)S(1)} copy-done((bf16[256,2048]{1,0:T(8,128)(2,1)S(1)}, bf16[256,2048]{1,0:T(8,128)(2,1)}, u32[]{:S(2)}) %copy-start) | copy-done | bytes 1048600
  3.5 0.0 copy-start.1
  3.5 1.2 %copy-done.1 = bf16[2048,256]{1,0:T(8,128)(2,1)S(1)} copy-done((bf16[2048,256]{1,0:T(8,128)(2,1)S(1)}, bf16[2048,256]{1,0:T(8,128)(2,1)}, u32[]{:S(2)}) %copy-start.1) | copy-done | bytes 1048600
  4.7 0.0 copy-start.2
  4.7 1.0 %copy-done.2 = bf16[256,1024]{1,0:T(8,128)(2,1)S(1)} copy-done((bf16[256,1024]{1,0:T(8,128)(2,1)S(1)}, bf16[256,1024]{1,0:T(8,128)(2,1)}, u32[]{:S(2)}) %copy-start.2) | copy-done | bytes 524312
  5.7 0.0 copy-start.3
  5.7 1.0 %copy-done.3 = bf16[256,1024]{1,0:T(8,128)(2,1)S(1)} copy-done((bf16[256,1024]{1,0:T(8,128)(2,1)S(1)}, bf16[256,1024]{1,0:T(8,128)(2,1)}, u32[]{:S(2)}) %copy-start.3) | copy-done | bytes 524312
  6.8 0.0 copy-start.4
  6.8 1.0 %copy-done.4 = bf16[1024,256]{1,0:T(8,128)(2,1)S(1)} copy-done((bf16[1024,256]{1,0:T(8,128)(2,1)S(1)}, bf16[1024,256]{1,0:T(8,128)(2,1)}, u32[]{:S(2)}) %copy-start.4) | copy-done | bytes 524312
  7.8 0.0 copy-start.5
  7.8 0.9 %copy-done.5 = bf16[256,512]{1,0:T(8,128)(2,1)S(1)} copy-done((bf16[256,512]{1,0:T(8,128)(2,1)S(1)}, bf16[256,512]{1,0:T(8,128)(2,1)}, u32[]{:S(2)}) %copy-start.5) | copy-done | bytes 262168
  8.8 0.0 copy-start.6
  8.8 0.9 %copy-done.6 = bf16[256,512]{1,0:T(8,128)(2,1)S(1)} copy-done((bf16[256,512]{1,0:T(8,128)(2,1)S(1)}, bf16[256,512]{1,0:T(8,128)(2,1)}, u32[]{:S(2)}) %copy-start.6) | copy-done | bytes 262168
  9.7 62.5 %layer.1 = (bf16[32,128]{1,0:T(8,128)(2,1)S(1)}, f32[8,2,256,512]{3,2,1,0:T(8,128)S(1)}) custom-call(bf16[128,32]{1,0:T(8,128)(2,1)S(1)} %copy.13.x_ref, bf16[16,128]{1,0:T(8,128)(2,1)S(1)} %pad.4.gains_ref, bf16[256,512]{1,0:T(8,128)(2,1)S(1)} %copy-done.5, bf16[256,512]{1,0:T(8,128)(2,1)S(1)} %copy-done.6, bf16[256,1024]{1,0:T(8,128)(2,1)S(1)} %copy-done.2, ...), custom_call_target="tpu_custom_call" | custom-call | tf_op jit(solution)/shard_map/layer/pallas_call | solution.py:244
  72.2 0.6 copy.16
  72.8 3.4 %copy.17 = f32[8,2,256,512]{3,2,1,0:T(8,128)} copy(f32[8,2,256,512]{3,2,1,0:T(8,128)S(1)} %get-tuple-element.9) | data formatting | bytes 16777216
  (2 shorter events, 0.0 us)
Async XLA Ops:
  2.2 1.2 %copy-start = (bf16[256,2048]{1,0:T(8,128)(2,1)S(1)}, bf16[256,2048]{1,0:T(8,128)(2,1)}, u32[]{:S(2)}) copy-start(bf16[256,2048]{1,0:T(8,128)(2,1)} %wu_ref.1) | copy-start | bytes 3145732
  3.5 1.2 %copy-start.1 = (bf16[2048,256]{1,0:T(8,128)(2,1)S(1)}, bf16[2048,256]{1,0:T(8,128)(2,1)}, u32[]{:S(2)}) copy-start(bf16[2048,256]{1,0:T(8,128)(2,1)} %wd_ref.1) | copy-start | bytes 3145732
  4.7 1.0 %copy-start.2 = (bf16[256,1024]{1,0:T(8,128)(2,1)S(1)}, bf16[256,1024]{1,0:T(8,128)(2,1)}, u32[]{:S(2)}) copy-start(bf16[256,1024]{1,0:T(8,128)(2,1)} %wv_ref.1) | copy-start | bytes 1572868
  5.7 1.0 %copy-start.3 = (bf16[256,1024]{1,0:T(8,128)(2,1)S(1)}, bf16[256,1024]{1,0:T(8,128)(2,1)}, u32[]{:S(2)}) copy-start(bf16[256,1024]{1,0:T(8,128)(2,1)} %wg_ref.1) | copy-start | bytes 1572868
  6.8 1.0 %copy-start.4 = (bf16[1024,256]{1,0:T(8,128)(2,1)S(1)}, bf16[1024,256]{1,0:T(8,128)(2,1)}, u32[]{:S(2)}) copy-start(bf16[1024,256]{1,0:T(8,128)(2,1)} %wo_ref.1) | copy-start | bytes 1572868
  7.8 0.9 %copy-start.5 = (bf16[256,512]{1,0:T(8,128)(2,1)S(1)}, bf16[256,512]{1,0:T(8,128)(2,1)}, u32[]{:S(2)}) copy-start(bf16[256,512]{1,0:T(8,128)(2,1)} %wq_ref.1) | copy-start | bytes 786436
  8.8 0.9 %copy-start.6 = (bf16[256,512]{1,0:T(8,128)(2,1)S(1)}, bf16[256,512]{1,0:T(8,128)(2,1)}, u32[]{:S(2)}) copy-start(bf16[256,512]{1,0:T(8,128)(2,1)} %wk_ref.1) | copy-start | bytes 786436

commit v2 on v0

v2 whole, which is shorter than its diff:
```python
import jax
import jax.numpy as jnp
from jax import lax
from jax.experimental import pallas as pl
from jax.experimental.pallas import tpu as pltpu
from jax.sharding import PartitionSpec as P

D = 4096
HEADS = 16
DK = 256
DV = 512
EPS = 1e-06
KV = 16
TP = 8
ROWS = 8
HPD = 2
NU = 4
UW = 2048 // NU
F32 = jnp.float32
BF16 = jnp.bfloat16
MESH = pl.DeviceIdType.MESH
HOPS = (0, 1, 2, 1)
PLANE = sorted(
    [(dz, dy) for dz in range(4) for dy in range(4) if dz or dy],
    key=lambda o: -(HOPS[o[0]] + HOPS[o[1]]),
)


def total(ref, n):
    acc = ref[0].astype(F32)
    for j in range(1, n):
        acc = acc + ref[j].astype(F32)
    return acc


def kernel(
    x_ref, mg_ref, cg_ref, wq_ref, wk_ref, wv_ref, wg_ref, wo_ref, wu_ref, wd_ref, state_ref,
    out_ref, st_ref,
    wq, wk, wv, wg, wo, wu, wd, gs,
    s1, r1, s1b, r1b, sq, rq, sk, rk, sv, rv, sg, rg, r4, s5, rd, r5, r6,
    su, ru, r7, s8, r8,
    xrows, qt, kt, ret, midt,
    lsem, ts, tr, ks, kr, plane,
):
    kv = lax.axis_index("kv")
    tp = lax.axis_index("tp")
    z, y = kv // 4, lax.rem(kv, 4)
    core, chip = lax.rem(tp, 2), tp // 2

    def plane_at(dz, dy):
        return lax.rem(z + dz, 4) * 4 + lax.rem(y + dy, 4)

    to = {o: plane_at(*o) for o in PLANE}
    come = {o: plane_at((4 - o[0]) % 4, (4 - o[1]) % 4) for o in PLANE}
    tpto = [lax.rem(tp + d, TP) for d in range(TP)]
    pair = tp + 1 - 2 * core
    sent = []

    def remote(src, dst, send, recv, device):
        return pltpu.make_async_remote_copy(
            src_ref=src, dst_ref=dst, send_sem=send, recv_sem=recv,
            device_id=device, device_id_type=MESH,
        )

    def go(copy):
        copy.start()
        sent.append(copy)

    def kv_scatter(c, s, r):
        for dz, dy in PLANE:
            o = dz * 4 + dy
            peer = to[dz, dy]
            go(remote(s.at[peer], r.at[o], ks.at[c, o], kr.at[c, o], {"kv": peer}))
        r[0] = s[kv]

    def kv_scattered(c, s, r):
        for dz, dy in PLANE:
            o = dz * 4 + dy
            remote(s.at[to[dz, dy]], r.at[o], ks.at[c, o], kr.at[c, o], {"kv": to[dz, dy]}).wait_recv()

    def kv_gather(c, r):
        for dz, dy in PLANE:
            o = dz * 4 + dy
            go(remote(r.at[kv], r.at[kv], ks.at[c, o], kr.at[c, o], {"kv": to[dz, dy]}))

    def kv_gathered(c, r):
        for dz, dy in PLANE:
            o = dz * 4 + dy
            slot = r.at[come[dz, dy]]
            remote(slot, slot, ks.at[c, o], kr.at[c, o], {"kv": to[dz, dy]}).wait_recv()

    barrier = pltpu.get_barrier_semaphore()
    ring = [{"kv": to[o]} for o in PLANE if 0 in o]
    for device in ring + [{"tp": p} for p in tpto[1:]]:
        pl.semaphore_signal(barrier, inc=1, device_id=device, device_id_type=MESH)
    first = [
        pltpu.make_async_copy(x_ref, s1b.at[0:32], lsem.at[8]),
        pltpu.make_async_copy(mg_ref, gs.at[0], lsem.at[9]),
        pltpu.make_async_copy(cg_ref, gs.at[1], lsem.at[10]),
    ]
    local = [
        pltpu.make_async_copy(a, b, lsem.at[i])
        for i, (a, b) in enumerate(
            ((wq_ref, wq), (wk_ref, wk), (wv_ref, wv), (wg_ref, wg), (state_ref, st_ref),
             (wo_ref, wo), (wu_ref, wu), (wd_ref, wd))
        )
    ]
    for c in first + local:
        c.start()
    for c in first:
        c.wait()

    r32 = lax.broadcasted_iota(jnp.int32, (32, 32), 0)
    c32 = lax.broadcasted_iota(jnp.int32, (32, 32), 1)
    column = jnp.sum(jnp.where(r32 == c32, gs[0].astype(F32), 0.0), axis=1, keepdims=True)
    s1[...] = (s1b[0:32, :].astype(F32) * column).astype(BF16)
    r1[tp] = s1[...]
    place = lax.broadcasted_iota(jnp.int32, (32, 128), 0) + 32 * lax.rem(tp, 4)
    place = jnp.where(place == lax.broadcasted_iota(jnp.int32, (32, 128), 1), 1.0, 0.0).astype(BF16)
    row = lax.broadcasted_iota(jnp.int32, (16, 32), 0)
    both = jnp.where(row == 0, gs[1].astype(F32), 0.0).astype(BF16)
    s1b[32:48, :] = jnp.dot(both, place, preferred_element_type=F32).astype(BF16)
    r1b[tp] = s1b[...]
    pl.semaphore_wait(barrier, len(ring) + TP - 1)

    for d in (5, 4, 3, 6, 2, 7, 1):
        go(remote(s1, r1.at[tp], ts.at[0, d], tr.at[0, d], {"tp": tpto[d]}))
    for d in (5, 4, 3, 6, 2, 7, 1):
        go(remote(s1b, r1b.at[tp], ts.at[1, d], tr.at[1, d], {"tp": tpto[d]}))
    for o in PLANE:
        if o[1] == 0:
            pl.semaphore_signal(plane, inc=1, device_id={"kv": to[o]}, device_id_type=MESH)
    for d in range(1, TP):
        remote(s1, r1.at[tpto[TP - d]], ts.at[0, d], tr.at[0, d], {"tp": tpto[d]}).wait_recv()
    normed = jnp.transpose(r1[...].astype(F32).reshape(256, 128)).astype(BF16)

    local[0].wait()
    sq[...] = jnp.dot(normed, wq[...], preferred_element_type=F32).astype(BF16).reshape(KV, ROWS, 512)
    pl.semaphore_wait(plane, 3)
    kv_scatter(0, sq, rq)
    local[1].wait()
    sk[...] = jnp.dot(normed, wk[...], preferred_element_type=F32).astype(BF16).reshape(KV, ROWS, 512)
    kv_scatter(1, sk, rk)
    for d in range(1, TP):
        remote(s1b, r1b.at[tpto[TP - d]], ts.at[1, d], tr.at[1, d], {"tp": tpto[d]}).wait_recv()
    x = jnp.transpose(jnp.concatenate([r1b[j, 0:32, :].astype(F32) for j in range(TP)], axis=0))
    xrows[...] = x.reshape(2, 64, 256)
    squares = jnp.sum(x * x, axis=1, keepdims=True)
    local[2].wait()
    sv[:, :, 0:1024] = jnp.dot(normed, wv[...], preferred_element_type=F32).astype(BF16).reshape(KV, ROWS, 1024)
    sv[:, :, 1024:1152] = jnp.broadcast_to(squares, (128, 128)).astype(BF16).reshape(KV, ROWS, 128)
    kv_scatter(2, sv, rv)
    local[3].wait()
    for h in range(HPD):
        part = jnp.dot(normed, wg[:, h * DV : (h + 1) * DV], preferred_element_type=F32)
        sg[h] = part.astype(BF16).reshape(KV, ROWS, DV)
        kv_scatter(3 + h, sg.at[h], rg.at[h])

    kv_scattered(0, sq, rq)
    query = total(rq, KV)
    qt[...] = jnp.transpose(query)
    kv_scattered(1, sk, rk)
    key = total(rk, KV)
    local[4].wait()
    for b in range(ROWS):
        for h in range(HPD):
            col = qt[h * DK : (h + 1) * DK, b : b + 1]
            ret[b : b + 1, h * DV : (h + 1) * DV] = jnp.sum(st_ref[b, h] * col, axis=0, keepdims=True)
    kv_scattered(2, sv, rv)
    sums = total(rv, KV)
    scale = lax.rsqrt(sums[:, 1024:1025] / D + EPS)
    value = scale * sums[:, 0:1024]
    query = scale * query
    key = scale * key * DK ** (-0.5)
    kt[...] = jnp.transpose(key)
    rates, outs = [], []
    for h in range(HPD):
        head = jnp.full((1, 128), (tp * HPD + h).astype(F32), F32)
        rates.append((1.0 - jnp.exp2(-1.0 - 6.0 * head / (HEADS - 1)))[:, 0:1])
        keys = slice(h * DK, (h + 1) * DK)
        cols = slice(h * DV, (h + 1) * DV)
        qk = jnp.sum(query[:, keys] * key[:, keys], axis=1, keepdims=True)
        out = rates[h] * (scale * ret[:, cols]) + qk * value[:, cols]
        outs.append(out * lax.rsqrt(jnp.mean(out * out, axis=1, keepdims=True) + EPS))
    for h in range(HPD):
        kv_scattered(3 + h, sg.at[h], rg.at[h])
        gate = scale * total(rg.at[h], KV)
        r4[h, kv] = (gate * jax.nn.sigmoid(gate) * outs[h]).astype(BF16)
        kv_gather(5 + h, r4.at[h])

    ret[...] = value
    for b in range(ROWS):
        for h in range(HPD):
            col = kt[h * DK : (h + 1) * DK, b : b + 1]
            st_ref[b, h] = rates[h] * st_ref[b, h] + col * ret[b : b + 1, h * DV : (h + 1) * DV]

    local[5].wait()
    terms = jnp.zeros((128, 256), F32)
    for h in range(HPD):
        kv_gathered(5 + h, r4.at[h])
        mixed = r4[h].astype(F32).reshape(128, DV).astype(BF16)
        terms = terms + jnp.dot(mixed, wo[h * DV : (h + 1) * DV, :], preferred_element_type=F32)
    s5[...] = terms.astype(BF16).reshape(2, 64, 256)
    swap = remote(s5.at[1 - core], rd, ts.at[2, 0], tr.at[2, 0], {"tp": pair})
    go(swap)
    swap.wait_recv()
    r5[chip] = (s5[core].astype(F32) + rd[...].astype(F32)).astype(BF16)
    for d in (4, 2, 6):
        go(remote(r5.at[chip], r5.at[chip], ts.at[2, d], tr.at[2, d], {"tp": tpto[d]}))
    for d in (2, 6, 4):
        slot = r5.at[tpto[TP - d] // 2]
        remote(slot, slot, ts.at[2, d], tr.at[2, d], {"tp": tpto[d]}).wait_recv()
    r6[core] = (xrows[core] + total(r5, 4)).astype(BF16)
    go(remote(r6.at[core], r6.at[core], ts.at[2, 1], tr.at[2, 1], {"tp": pair}))
    local[6].wait()
    remote(r6.at[1 - core], r6.at[1 - core], ts.at[2, 1], tr.at[2, 1], {"tp": pair}).wait_recv()
    middle = r6[...].astype(F32).reshape(128, 256)
    gains = jnp.concatenate(
        [sum(r1b[j, 32:48, :].astype(F32) for j in range(4 * i, 4 * i + 4)) for i in range(2)], axis=1
    )
    cnormed = (middle * gains[0:1, :]).astype(BF16)

    for c in range(NU):
        if c == 0:
            msquares = jnp.sum(middle * middle, axis=1, keepdims=True)
            su[0, :, :, UW : UW + 128] = jnp.broadcast_to(msquares, (128, 128)).astype(BF16).reshape(KV, ROWS, 128)
        part = jnp.dot(cnormed, wu[:, c * UW : (c + 1) * UW], preferred_element_type=F32)
        su[c, :, :, 0:UW] = part.astype(BF16).reshape(KV, ROWS, UW)
        if c == 0:
            kv_scatter(7, su.at[0], ru.at[0])
        else:
            kv_scatter(7 + c, su.at[c, :, :, 0:UW], ru.at[c, :, :, 0:UW])
    midt[...] = jnp.transpose(middle)
    for c in range(NU):
        if c == 0:
            kv_scattered(7, su.at[0], ru.at[0])
        else:
            kv_scattered(7 + c, su.at[c, :, :, 0:UW], ru.at[c, :, :, 0:UW])
        if c == 0:
            up = total(ru.at[0], KV)
            cscale = lax.rsqrt(up[:, UW : UW + 1] / D + EPS)
            up = up[:, 0:UW]
        else:
            up = total(ru.at[c, :, :, 0:UW], KV)
        r7[c, kv] = jnp.square(jnp.maximum(cscale * up, 0.0)).astype(BF16)
        kv_gather(7 + NU + c, r7.at[c])

    local[7].wait()
    down = jnp.zeros((128, 256), F32)
    for c in range(NU):
        kv_gathered(7 + NU + c, r7.at[c])
        hidden = r7[c].astype(F32).reshape(128, UW).astype(BF16)
        down = down + jnp.dot(hidden, wd[c * UW : (c + 1) * UW, :], preferred_element_type=F32)
    s8[...] = jnp.transpose(down).astype(BF16).reshape(TP, 32, 128)
    for d in (5, 4, 3, 6, 2, 7, 1):
        go(remote(s8.at[tpto[d]], r8.at[d], ts.at[3, d], tr.at[3, d], {"tp": tpto[d]}))
    r8[0] = s8[tp]
    for d in range(1, TP):
        remote(s8.at[tpto[d]], r8.at[d], ts.at[3, d], tr.at[3, d], {"tp": tpto[d]}).wait_recv()
    lowered = total(r8, TP)
    out_ref[...] = (midt[pl.ds(pl.multiple_of(tp * 32, 32), 32), :] + lowered).astype(BF16)
    for copy in sent:
        copy.wait_send()


def writer(a_ref, s_ref, out_ref, state_ref, sem):
    copies = [pltpu.make_async_copy(a_ref, out_ref, sem.at[ROWS])]
    copies += [pltpu.make_async_copy(s_ref.at[b], state_ref.at[b], sem.at[b]) for b in range(ROWS)]
    for c in copies:
        c.start()
    for c in copies:
        c.wait()


def per_device(x, mixer_gain, channel_gain, wq, wk, wv, wg, wo, wu, wd, state):
    vm = pl.BlockSpec(memory_space=pltpu.VMEM)
    hb = pl.BlockSpec(memory_space=pltpu.HBM)
    dma = pltpu.SemaphoreType.DMA
    v = lambda *shape: pltpu.VMEM(shape, BF16)
    f = lambda *shape: pltpu.VMEM(shape, F32)
    scratch = [
        v(256, 512), v(256, 512), v(256, 1024), v(256, 1024), v(1024, 256), v(256, 2048), v(2048, 256), v(2, 1, 32),
        v(32, 128), v(TP, 32, 128), v(48, 128), v(TP, 48, 128),
        v(KV, ROWS, 512), v(KV, ROWS, 512), v(KV, ROWS, 512), v(KV, ROWS, 512),
        v(KV, ROWS, 1152), v(KV, ROWS, 1152), v(HPD, KV, ROWS, DV), v(HPD, KV, ROWS, DV),
        v(HPD, KV, ROWS, DV), v(2, 64, 256), v(64, 256), v(4, 64, 256), v(2, 64, 256),
        v(NU, KV, ROWS, UW + 128), v(NU, KV, ROWS, UW + 128), v(NU, KV, ROWS, UW),
        v(TP, 32, 128), v(TP, 32, 128),
        f(2, 64, 256), f(512, ROWS), f(512, ROWS), f(ROWS, 1024), f(256, 128),
        dma((11,)), dma((4, TP)), dma((4, TP)), dma((7 + 2 * NU, KV)), dma((7 + 2 * NU, KV)),
        pltpu.SemaphoreType.REGULAR,
    ]
    out, new_state = pl.pallas_call(
        kernel,
        name="layer",
        out_shape=(pltpu.VMEM((32, 128), BF16), pltpu.VMEM(state.shape, F32)),
        in_specs=[hb] * 11,
        out_specs=(vm, vm),
        scratch_shapes=scratch,
        compiler_params=pltpu.CompilerParams(
            collective_id=0, has_side_effects=True, vmem_limit_bytes=int(55.7 * 2**20)
        ),
    )(x.T, mixer_gain.reshape(1, 32), channel_gain.reshape(1, 32), wq, wk, wv, wg, wo, wu, wd, state)
    out, new_state = pl.pallas_call(
        writer,
        name="writer",
        out_shape=(jax.ShapeDtypeStruct((32, 128), BF16), jax.ShapeDtypeStruct(state.shape, F32)),
        in_specs=[vm, vm],
        out_specs=(hb, hb),
        scratch_shapes=[dma((ROWS + 1,))],
        compiler_params=pltpu.CompilerParams(vmem_limit_bytes=2**20),
    )(out, new_state)
    return out.T, new_state


def solution(mesh):
    return jax.shard_map(
        per_device,
        mesh=mesh,
        in_specs=(
            P(None, ("kv", "tp")),
            P(("kv", "tp")),
            P(("kv", "tp")),
            P("kv", "tp"),
            P("kv", "tp"),
            P("kv", "tp"),
            P("kv", "tp"),
            P("tp", "kv"),
            P("kv", "tp"),
            P("tp", "kv"),
            P("kv", "tp", None, None),
        ),
        out_specs=(P(None, ("kv", "tp")), P("kv", "tp", None, None)),
        check_vma=False,
    )
```

time: 143 us -> 62.3 us (0.44)
  blocking collectives: 65.5 us -> 0 us
  Pallas kernels: 0 us -> 61.5 us
  waiting for transfers between devices: 27.5 us -> 0 us
  starting transfers between devices: 21.2 us -> 0 us
  matrix products: 12.6 us -> 0 us
  other arithmetic: 7.36 us -> 0 us
  local copies, waits for them, and re-layouts: 6.76 us -> 0 us
    all_to_all x6 -> x0, blocking collectives: 65.5 us -> none  [the longest x4 41.5 us: sent_to_all(): lax.all_to_all(jnp.broadcast_to(value[None], (size, *value.shape)), axis,...]
    pallas_call x0 -> x2, Pallas kernels: none -> 61.5 us  [the longest x1 58.1 us: per_device(): pl.pallas_call(kernel, name='layer', out_shape=(pltpu.VMEM((32, 128), BF1...]
    all_to_all x4 -> x0, waiting for transfers between devices: 27.5 us -> none  [the longest x2 18.2 us: sum_at_owner(): parts = lax.all_to_all(split_up(value, dim, size), axis, 0, 0, tiled=True)]
    all_to_all x4 -> x0, starting transfers between devices: 21.2 us -> none  [the longest x2 13.3 us: sum_at_owner(): parts = lax.all_to_all(split_up(value, dim, size), axis, 0, 0, tiled=True)]
    dot_general x8 -> x0, matrix products: 12.6 us -> none  [the longest x1 4.05 us: retain(): jnp.einsum('shd,shde->she', query, new_state, precision=lax.Precision.HIG...]
    add x1 -> x0, other arithmetic: 4.08 us -> none  [retain(): rates[None, :, None, None] * old_state]
    unnamed x12 -> x0, local copies, waits for them, and re-layouts: 3.39 us -> none
    convert_element_type x7 -> x0, other arithmetic: 1.61 us -> none  [the longest x1 0.75 us: per_device(): normed = (stream * mixer_gain.astype(jnp.float32)).astype(jnp.bfloat16)]
  transfers between devices with their start and end apart: 4 -> 0, of which waited for: 4 -> 0; matrix products, arithmetic and copies ran while one was open for 0% -> 0% of each run, Pallas kernels for 0% -> 0%
where the time goes in v2:
time: 62.3 us; the launch traced here: 62.2 us
  Pallas kernels  61.5 us (99%)
  between operations  0.64 us (1%)
    pallas_call x1, Pallas kernels, per_device(): pl.pallas_call(kernel, name='layer', out_shape=(pltpu.VMEM((32, 128), BF1...  58.1 us
    pallas_call x1, Pallas kernels, per_device(): pl.pallas_call(writer, name='writer', out_shape=(jax.ShapeDtypeStruct((32...  3.38 us

profile of v2, /device:TPU:1, one launch (start us, length us, event | category | flops | bytes accessed | tf_op | source)
XLA Modules:
  0.0 62.2 jit_solution(599039793383997686)
XLA Ops:
  0.6 58.1 %layer.1 = (bf16[32,128]{1,0:T(8,128)(2,1)S(1)}, f32[8,2,256,512]{3,2,1,0:T(8,128)S(1)}) custom-call(bf16[32,128]{1,0:T(8,128)(2,1)} %bitcast.4, bf16[1,32]{1,0:T(2,128)(2,1)} %bitcast.5, bf16[1,32]{1,0:T(2,128)(2,1)} %bitcast.6, bf16[256,512]{1,0:T(8,128)(2,1)} %wq_ref.1, bf16[256,512]{1,0:T(8,128)(2,1)} %wk_ref.1, bf16[256,1024]{1,0:T(8,128)(2,1)} %wv_ref.1, ...), custom_call_target="tpu_custom_call" | custom-call | tf_op jit(solution)/shard_map/layer/pallas_call | solution.py:293
  58.8 3.4 %writer.1 = (bf16[32,128]{1,0:T(8,128)(2,1)}, f32[8,2,256,512]{3,2,1,0:T(8,128)}) custom-call(bf16[32,128]{1,0:T(8,128)(2,1)S(1)} %get-tuple-element.6.a_ref, f32[8,2,256,512]{3,2,1,0:T(8,128)S(1)} %get-tuple-element.7.s_ref), custom_call_target="tpu_custom_call" | custom-call | tf_op jit(solution)/shard_map/writer/pallas_call | solution.py:304

commit v3 on v2

--- a/solution.py
+++ b/solution.py
@@ -51,7 +51,6 @@
         return lax.rem(z + dz, 4) * 4 + lax.rem(y + dy, 4)
 
     to = {o: plane_at(*o) for o in PLANE}
-    come = {o: plane_at((4 - o[0]) % 4, (4 - o[1]) % 4) for o in PLANE}
     tpto = [lax.rem(tp + d, TP) for d in range(TP)]
     pair = tp + 1 - 2 * core
     sent = []
@@ -62,32 +61,25 @@
             device_id=device, device_id_type=MESH,
         )
 
-    def go(copy):
-        copy.start()
-        sent.append(copy)
+    def step(sems, i, slots, device):
+        whole = remote(slots, slots, sems[0].at[i], sems[1].at[i], device)
+        sent.append(whole)
+        return whole
+
+    ksem, tsem = (ks, kr), (ts, tr)
+    aside, across = {"kv": to[0, 1]}, {"tp": tpto[1]}
 
     def kv_scatter(c, s, r):
         for dz, dy in PLANE:
-            o = dz * 4 + dy
             peer = to[dz, dy]
-            go(remote(s.at[peer], r.at[o], ks.at[c, o], kr.at[c, o], {"kv": peer}))
+            remote(s.at[peer], r.at[dz * 4 + dy], ks.at[c], kr.at[c], {"kv": peer}).start()
         r[0] = s[kv]
-
-    def kv_scattered(c, s, r):
-        for dz, dy in PLANE:
-            o = dz * 4 + dy
-            remote(s.at[to[dz, dy]], r.at[o], ks.at[c, o], kr.at[c, o], {"kv": to[dz, dy]}).wait_recv()
+        return step(ksem, c, r.at[1:KV], aside)
 
     def kv_gather(c, r):
-        for dz, dy in PLANE:
-            o = dz * 4 + dy
-            go(remote(r.at[kv], r.at[kv], ks.at[c, o], kr.at[c, o], {"kv": to[dz, dy]}))
-
-    def kv_gathered(c, r):
-        for dz, dy in PLANE:
-            o = dz * 4 + dy
-            slot = r.at[come[dz, dy]]
-            remote(slot, slot, ks.at[c, o], kr.at[c, o], {"kv": to[dz, dy]}).wait_recv()
+        for o in PLANE:
+            remote(r.at[kv], r.at[kv], ks.at[c], kr.at[c], {"kv": to[o]}).start()
+        return step(ksem, c, r.at[1:KV], aside)
 
     barrier = pltpu.get_barrier_semaphore()
     ring = [{"kv": to[o]} for o in PLANE if 0 in o]
@@ -124,49 +116,50 @@
     pl.semaphore_wait(barrier, len(ring) + TP - 1)
 
     for d in (5, 4, 3, 6, 2, 7, 1):
-        go(remote(s1, r1.at[tp], ts.at[0, d], tr.at[0, d], {"tp": tpto[d]}))
+        remote(s1, r1.at[tp], ts.at[0], tr.at[0], {"tp": tpto[d]}).start()
     for d in (5, 4, 3, 6, 2, 7, 1):
-        go(remote(s1b, r1b.at[tp], ts.at[1, d], tr.at[1, d], {"tp": tpto[d]}))
+        remote(s1b, r1b.at[tp], ts.at[1], tr.at[1], {"tp": tpto[d]}).start()
+    first_in = step(tsem, 0, r1.at[1:TP], across)
+    second_in = step(tsem, 1, r1b.at[1:TP], across)
     for o in PLANE:
         if o[1] == 0:
             pl.semaphore_signal(plane, inc=1, device_id={"kv": to[o]}, device_id_type=MESH)
-    for d in range(1, TP):
-        remote(s1, r1.at[tpto[TP - d]], ts.at[0, d], tr.at[0, d], {"tp": tpto[d]}).wait_recv()
+    first_in.wait_recv()
     normed = jnp.transpose(r1[...].astype(F32).reshape(256, 128)).astype(BF16)
 
     local[0].wait()
     sq[...] = jnp.dot(normed, wq[...], preferred_element_type=F32).astype(BF16).reshape(KV, ROWS, 512)
     pl.semaphore_wait(plane, 3)
-    kv_scatter(0, sq, rq)
+    query_in = kv_scatter(0, sq, rq)
     local[1].wait()
     sk[...] = jnp.dot(normed, wk[...], preferred_element_type=F32).astype(BF16).reshape(KV, ROWS, 512)
-    kv_scatter(1, sk, rk)
-    for d in range(1, TP):
-        remote(s1b, r1b.at[tpto[TP - d]], ts.at[1, d], tr.at[1, d], {"tp": tpto[d]}).wait_recv()
+    key_in = kv_scatter(1, sk, rk)
+    second_in.wait_recv()
     x = jnp.transpose(jnp.concatenate([r1b[j, 0:32, :].astype(F32) for j in range(TP)], axis=0))
     xrows[...] = x.reshape(2, 64, 256)
     squares = jnp.sum(x * x, axis=1, keepdims=True)
     local[2].wait()
     sv[:, :, 0:1024] = jnp.dot(normed, wv[...], preferred_element_type=F32).astype(BF16).reshape(KV, ROWS, 1024)
     sv[:, :, 1024:1152] = jnp.broadcast_to(squares, (128, 128)).astype(BF16).reshape(KV, ROWS, 128)
-    kv_scatter(2, sv, rv)
+    value_in = kv_scatter(2, sv, rv)
     local[3].wait()
+    gate_in, mixed_in = [], []
     for h in range(HPD):
         part = jnp.dot(normed, wg[:, h * DV : (h + 1) * DV], preferred_element_type=F32)
         sg[h] = part.astype(BF16).reshape(KV, ROWS, DV)
-        kv_scatter(3 + h, sg.at[h], rg.at[h])
-
-    kv_scattered(0, sq, rq)
+        gate_in.append(kv_scatter(3 + h, sg.at[h], rg.at[h]))
+
+    query_in.wait_recv()
     query = total(rq, KV)
     qt[...] = jnp.transpose(query)
-    kv_scattered(1, sk, rk)
+    key_in.wait_recv()
     key = total(rk, KV)
     local[4].wait()
     for b in range(ROWS):
         for h in range(HPD):
             col = qt[h * DK : (h + 1) * DK, b : b + 1]
             ret[b : b + 1, h * DV : (h + 1) * DV] = jnp.sum(st_ref[b, h] * col, axis=0, keepdims=True)
-    kv_scattered(2, sv, rv)
+    value_in.wait_recv()
     sums = total(rv, KV)
     scale = lax.rsqrt(sums[:, 1024:1025] / D + EPS)
     value = scale * sums[:, 0:1024]
@@ -183,10 +176,10 @@
         out = rates[h] * (scale * ret[:, cols]) + qk * value[:, cols]
         outs.append(out * lax.rsqrt(jnp.mean(out * out, axis=1, keepdims=True) + EPS))
     for h in range(HPD):
-        kv_scattered(3 + h, sg.at[h], rg.at[h])
+        gate_in[h].wait_recv()
         gate = scale * total(rg.at[h], KV)
         r4[h, kv] = (gate * jax.nn.sigmoid(gate) * outs[h]).astype(BF16)
-        kv_gather(5 + h, r4.at[h])
+        mixed_in.append(kv_gather(5 + h, r4.at[h]))
 
     ret[...] = value
     for b in range(ROWS):
@@ -197,45 +190,39 @@
     local[5].wait()
     terms = jnp.zeros((128, 256), F32)
     for h in range(HPD):
-        kv_gathered(5 + h, r4.at[h])
+        mixed_in[h].wait_recv()
         mixed = r4[h].astype(F32).reshape(128, DV).astype(BF16)
         terms = terms + jnp.dot(mixed, wo[h * DV : (h + 1) * DV, :], preferred_element_type=F32)
     s5[...] = terms.astype(BF16).reshape(2, 64, 256)
-    swap = remote(s5.at[1 - core], rd, ts.at[2, 0], tr.at[2, 0], {"tp": pair})
-    go(swap)
-    swap.wait_recv()
+    mate = {"tp": pair}
+    remote(s5.at[1 - core], rd, ts.at[2], tr.at[2], mate).start()
+    step(tsem, 2, rd, mate).wait_recv()
     r5[chip] = (s5[core].astype(F32) + rd[...].astype(F32)).astype(BF16)
     for d in (4, 2, 6):
-        go(remote(r5.at[chip], r5.at[chip], ts.at[2, d], tr.at[2, d], {"tp": tpto[d]}))
-    for d in (2, 6, 4):
-        slot = r5.at[tpto[TP - d] // 2]
-        remote(slot, slot, ts.at[2, d], tr.at[2, d], {"tp": tpto[d]}).wait_recv()
+        remote(r5.at[chip], r5.at[chip], ts.at[3], tr.at[3], {"tp": tpto[d]}).start()
+    step(tsem, 3, r5.at[1:4], across).wait_recv()
     r6[core] = (xrows[core] + total(r5, 4)).astype(BF16)
-    go(remote(r6.at[core], r6.at[core], ts.at[2, 1], tr.at[2, 1], {"tp": pair}))
+    remote(r6.at[core], r6.at[core], ts.at[4], tr.at[4], mate).start()
     local[6].wait()
-    remote(r6.at[1 - core], r6.at[1 - core], ts.at[2, 1], tr.at[2, 1], {"tp": pair}).wait_recv()
+    step(tsem, 4, r6.at[1 - core], mate).wait_recv()
     middle = r6[...].astype(F32).reshape(128, 256)
     gains = jnp.concatenate(
         [sum(r1b[j, 32:48, :].astype(F32) for j in range(4 * i, 4 * i + 4)) for i in range(2)], axis=1
     )
     cnormed = (middle * gains[0:1, :]).astype(BF16)
 
+    up_in, hidden_in = [], []
     for c in range(NU):
         if c == 0:
             msquares = jnp.sum(middle * middle, axis=1, keepdims=True)
             su[0, :, :, UW : UW + 128] = jnp.broadcast_to(msquares, (128, 128)).astype(BF16).reshape(KV, ROWS, 128)
         part = jnp.dot(cnormed, wu[:, c * UW : (c + 1) * UW], preferred_element_type=F32)
         su[c, :, :, 0:UW] = part.astype(BF16).reshape(KV, ROWS, UW)
-        if c == 0:
-            kv_scatter(7, su.at[0], ru.at[0])
-        else:
-            kv_scatter(7 + c, su.at[c, :, :, 0:UW], ru.at[c, :, :, 0:UW])
+        width = UW + 128 if c == 0 else UW
+        up_in.append(kv_scatter(7 + c, su.at[c, :, :, 0:width], ru.at[c, :, :, 0:width]))
     midt[...] = jnp.transpose(middle)
     for c in range(NU):
-        if c == 0:
-            kv_scattered(7, su.at[0], ru.at[0])
-        else:
-            kv_scattered(7 + c, su.at[c, :, :, 0:UW], ru.at[c, :, :, 0:UW])
+        up_in[c].wait_recv()
         if c == 0:
             up = total(ru.at[0], KV)
             cscale = lax.rsqrt(up[:, UW : UW + 1] / D + EPS)
@@ -243,20 +230,19 @@
         else:
             up = total(ru.at[c, :, :, 0:UW], KV)
         r7[c, kv] = jnp.square(jnp.maximum(cscale * up, 0.0)).astype(BF16)
-        kv_gather(7 + NU + c, r7.at[c])
+        hidden_in.append(kv_gather(7 + NU + c, r7.at[c]))
 
     local[7].wait()
     down = jnp.zeros((128, 256), F32)
     for c in range(NU):
-        kv_gathered(7 + NU + c, r7.at[c])
+        hidden_in[c].wait_recv()
         hidden = r7[c].astype(F32).reshape(128, UW).astype(BF16)
         down = down + jnp.dot(hidden, wd[c * UW : (c + 1) * UW, :], preferred_element_type=F32)
     s8[...] = jnp.transpose(down).astype(BF16).reshape(TP, 32, 128)
     for d in (5, 4, 3, 6, 2, 7, 1):
-        go(remote(s8.at[tpto[d]], r8.at[d], ts.at[3, d], tr.at[3, d], {"tp": tpto[d]}))
+        remote(s8.at[tpto[d]], r8.at[d], ts.at[5], tr.at[5], {"tp": tpto[d]}).start()
     r8[0] = s8[tp]
-    for d in range(1, TP):
-        remote(s8.at[tpto[d]], r8.at[d], ts.at[3, d], tr.at[3, d], {"tp": tpto[d]}).wait_recv()
+    step(tsem, 5, r8.at[1:TP], across).wait_recv()
     lowered = total(r8, TP)
     out_ref[...] = (midt[pl.ds(pl.multiple_of(tp * 32, 32), 32), :] + lowered).astype(BF16)
     for copy in sent:
@@ -287,7 +273,7 @@
         v(NU, KV, ROWS, UW + 128), v(NU, KV, ROWS, UW + 128), v(NU, KV, ROWS, UW),
         v(TP, 32, 128), v(TP, 32, 128),
         f(2, 64, 256), f(512, ROWS), f(512, ROWS), f(ROWS, 1024), f(256, 128),
-        dma((11,)), dma((4, TP)), dma((4, TP)), dma((7 + 2 * NU, KV)), dma((7 + 2 * NU, KV)),
+        dma((11,)), dma((6,)), dma((6,)), dma((7 + 2 * NU,)), dma((7 + 2 * NU,)),
         pltpu.SemaphoreType.REGULAR,
     ]
     out, new_state = pl.pallas_call(

time: 62.3 us -> 57.4 us (0.921)
  Pallas kernels: 61.5 us -> 56.6 us
    pallas_call x1, Pallas kernels: 58.1 us -> 53.3 us  [per_device(): pl.pallas_call(kernel, name='layer', out_shape=(pltpu.VMEM((32, 128), BF1...]
where the time goes in v3:
time: 57.4 us; the launch traced here: 57.3 us
  Pallas kernels  56.6 us (99%)
  between operations  0.64 us (1%)
    pallas_call x1, Pallas kernels, per_device(): pl.pallas_call(kernel, name='layer', out_shape=(pltpu.VMEM((32, 128), BF1...  53.3 us
    pallas_call x1, Pallas kernels, per_device(): pl.pallas_call(writer, name='writer', out_shape=(jax.ShapeDtypeStruct((32...  3.38 us

profile of v3, /device:TPU:1, one launch (start us, length us, event | category | flops | bytes accessed | tf_op | source)
XLA Modules:
  0.0 57.3 jit_solution(8623258408623916310)
XLA Ops:
  0.6 53.3 %layer.1 = (bf16[32,128]{1,0:T(8,128)(2,1)S(1)}, f32[8,2,256,512]{3,2,1,0:T(8,128)S(1)}) custom-call(bf16[32,128]{1,0:T(8,128)(2,1)} %bitcast.4, bf16[1,32]{1,0:T(2,128)(2,1)} %bitcast.5, bf16[1,32]{1,0:T(2,128)(2,1)} %bitcast.6, bf16[256,512]{1,0:T(8,128)(2,1)} %wq_ref.1, bf16[256,512]{1,0:T(8,128)(2,1)} %wk_ref.1, bf16[256,1024]{1,0:T(8,128)(2,1)} %wv_ref.1, ...), custom_call_target="tpu_custom_call" | custom-call | tf_op jit(solution)/shard_map/layer/pallas_call | solution.py:279
  53.9 3.4 %writer.1 = (bf16[32,128]{1,0:T(8,128)(2,1)}, f32[8,2,256,512]{3,2,1,0:T(8,128)}) custom-call(bf16[32,128]{1,0:T(8,128)(2,1)S(1)} %get-tuple-element.6.a_ref, f32[8,2,256,512]{3,2,1,0:T(8,128)S(1)} %get-tuple-element.7.s_ref), custom_call_target="tpu_custom_call" | custom-call | tf_op jit(solution)/shard_map/writer/pallas_call | solution.py:290

commit v4 on v3

--- a/solution.py
+++ b/solution.py
@@ -37,9 +37,9 @@
     x_ref, mg_ref, cg_ref, wq_ref, wk_ref, wv_ref, wg_ref, wo_ref, wu_ref, wd_ref, state_ref,
     out_ref, st_ref,
     wq, wk, wv, wg, wo, wu, wd, gs,
-    s1, r1, s1b, r1b, sq, rq, sk, rk, sv, rv, sg, rg, r4, s5, rd, r5, r6,
+    s1, r1, s1b, r1b, sq, rq, tq, uq, sk, rk, tk, uk, sv, rv, tv, uv, sg, rg, tg, ug, r4, s5, rd, r5, r6,
     su, ru, r7, s8, r8,
-    xrows, qt, kt, ret, midt,
+    xrows, tacc, qt, kt, ret, midt,
     lsem, ts, tr, ks, kr, plane,
 ):
     kv = lax.axis_index("kv")
@@ -69,12 +69,26 @@
     ksem, tsem = (ks, kr), (ts, tr)
     aside, across = {"kv": to[0, 1]}, {"tp": tpto[1]}
 
-    def kv_scatter(c, s, r):
-        for dz, dy in PLANE:
-            peer = to[dz, dy]
-            remote(s.at[peer], r.at[dz * 4 + dy], ks.at[c], kr.at[c], {"kv": peer}).start()
-        r[0] = s[kv]
-        return step(ksem, c, r.at[1:KV], aside)
+    ring_at = {"z": (z, lambda q: {"kv": q * 4 + y}), "y": (y, lambda q: {"kv": z * 4 + q})}
+
+    def ring_scatter(c, axis, s, r):
+        me, device = ring_at[axis]
+        part = (lambda q: s.at[q]) if axis == "z" else (lambda q: s.at[:, q])
+        for d in (2, 1, 3):
+            q = lax.rem(me + d, 4)
+            remote(part(q), r.at[d], ks.at[c], kr.at[c], device(q)).start()
+        r[0] = part(me)[...]
+        return step(ksem, c, r.at[1:4], aside)
+
+    def ring_finish(stage, c, axis, r, t, u):
+        me, device = ring_at[axis]
+        stage.wait_recv()
+        t[...] = total(r, 4).astype(BF16)
+        for d in (2, 1, 3):
+            q = lax.rem(me + d, 4)
+            remote(t.at[q], u.at[d], ks.at[c], kr.at[c], device(q)).start()
+        u[0] = t[me]
+        return step(ksem, c, u.at[1:4], aside)
 
     def kv_gather(c, r):
         for o in PLANE:
@@ -128,39 +142,44 @@
     normed = jnp.transpose(r1[...].astype(F32).reshape(256, 128)).astype(BF16)
 
     local[0].wait()
-    sq[...] = jnp.dot(normed, wq[...], preferred_element_type=F32).astype(BF16).reshape(KV, ROWS, 512)
+    sq[...] = jnp.dot(normed, wq[...], preferred_element_type=F32).reshape(4, 4, ROWS, 512).astype(BF16)
     pl.semaphore_wait(plane, 3)
-    query_in = kv_scatter(0, sq, rq)
+    query_in = ring_scatter(0, "z", sq, rq)
     local[1].wait()
-    sk[...] = jnp.dot(normed, wk[...], preferred_element_type=F32).astype(BF16).reshape(KV, ROWS, 512)
-    key_in = kv_scatter(1, sk, rk)
+    sk[...] = jnp.dot(normed, wk[...], preferred_element_type=F32).reshape(4, 4, ROWS, 512).astype(BF16)
+    key_in = ring_scatter(1, "z", sk, rk)
     second_in.wait_recv()
     x = jnp.transpose(jnp.concatenate([r1b[j, 0:32, :].astype(F32) for j in range(TP)], axis=0))
     xrows[...] = x.reshape(2, 64, 256)
     squares = jnp.sum(x * x, axis=1, keepdims=True)
     local[2].wait()
-    sv[:, :, 0:1024] = jnp.dot(normed, wv[...], preferred_element_type=F32).astype(BF16).reshape(KV, ROWS, 1024)
-    sv[:, :, 1024:1152] = jnp.broadcast_to(squares, (128, 128)).astype(BF16).reshape(KV, ROWS, 128)
-    value_in = kv_scatter(2, sv, rv)
+    sv[:, :, :, 0:1024] = jnp.dot(normed, wv[...], preferred_element_type=F32).reshape(4, 4, ROWS, 1024).astype(BF16)
+    sv[:, :, :, 1024:1152] = jnp.broadcast_to(squares, (128, 128)).reshape(4, 4, ROWS, 128).astype(BF16)
+    value_in = ring_scatter(2, "y", sv, rv)
     local[3].wait()
     gate_in, mixed_in = [], []
     for h in range(HPD):
         part = jnp.dot(normed, wg[:, h * DV : (h + 1) * DV], preferred_element_type=F32)
-        sg[h] = part.astype(BF16).reshape(KV, ROWS, DV)
-        gate_in.append(kv_scatter(3 + h, sg.at[h], rg.at[h]))
-
+        sg[h] = part.reshape(4, 4, ROWS, DV).astype(BF16)
+        gate_in.append(ring_scatter(3 + h, "zy"[h], sg.at[h], rg.at[h]))
+
+    query_in = ring_finish(query_in, 7 + 2 * NU, "y", rq, tq, uq)
+    key_in = ring_finish(key_in, 7 + 2 * NU + 1, "y", rk, tk, uk)
+    value_in = ring_finish(value_in, 7 + 2 * NU + 2, "z", rv, tv, uv)
+    for h in range(HPD):
+        gate_in[h] = ring_finish(gate_in[h], 10 + 2 * NU + h, "yz"[h], rg.at[h], tg.at[h], ug.at[h])
     query_in.wait_recv()
-    query = total(rq, KV)
+    query = total(uq, 4)
     qt[...] = jnp.transpose(query)
     key_in.wait_recv()
-    key = total(rk, KV)
+    key = total(uk, 4)
     local[4].wait()
     for b in range(ROWS):
         for h in range(HPD):
             col = qt[h * DK : (h + 1) * DK, b : b + 1]
             ret[b : b + 1, h * DV : (h + 1) * DV] = jnp.sum(st_ref[b, h] * col, axis=0, keepdims=True)
     value_in.wait_recv()
-    sums = total(rv, KV)
+    sums = total(uv, 4)
     scale = lax.rsqrt(sums[:, 1024:1025] / D + EPS)
     value = scale * sums[:, 0:1024]
     query = scale * query
@@ -177,7 +196,7 @@
         outs.append(out * lax.rsqrt(jnp.mean(out * out, axis=1, keepdims=True) + EPS))
     for h in range(HPD):
         gate_in[h].wait_recv()
-        gate = scale * total(rg.at[h], KV)
+        gate = scale * total(ug.at[h], 4)
         r4[h, kv] = (gate * jax.nn.sigmoid(gate) * outs[h]).astype(BF16)
         mixed_in.append(kv_gather(5 + h, r4.at[h]))
 
@@ -188,38 +207,73 @@
             st_ref[b, h] = rates[h] * st_ref[b, h] + col * ret[b : b + 1, h * DV : (h + 1) * DV]
 
     local[5].wait()
-    terms = jnp.zeros((128, 256), F32)
-    for h in range(HPD):
-        mixed_in[h].wait_recv()
-        mixed = r4[h].astype(F32).reshape(128, DV).astype(BF16)
-        terms = terms + jnp.dot(mixed, wo[h * DV : (h + 1) * DV, :], preferred_element_type=F32)
-    s5[...] = terms.astype(BF16).reshape(2, 64, 256)
+    mixed_in[0].wait_recv()
+    mixed = r4[0].astype(F32).reshape(128, DV).astype(BF16)
+    tacc[...] = jnp.dot(mixed, wo[0:DV, :], preferred_element_type=F32).reshape(2, 64, 256)
+    mixed_in[1].wait_recv()
+
+    def half_terms(half):
+        rows = r4[1, pl.ds(half * 8, 8)].astype(F32).reshape(64, DV).astype(BF16)
+        return tacc[half] + jnp.dot(rows, wo[DV : 2 * DV, :], preferred_element_type=F32)
+
     mate = {"tp": pair}
-    remote(s5.at[1 - core], rd, ts.at[2], tr.at[2], mate).start()
+    s5[...] = half_terms(1 - core).astype(BF16)
+    remote(s5, rd, ts.at[2], tr.at[2], mate).start()
+    kept = half_terms(core)
     step(tsem, 2, rd, mate).wait_recv()
-    r5[chip] = (s5[core].astype(F32) + rd[...].astype(F32)).astype(BF16)
+    r5[chip] = (kept + rd[...].astype(F32)).astype(BF16)
     for d in (4, 2, 6):
         remote(r5.at[chip], r5.at[chip], ts.at[3], tr.at[3], {"tp": tpto[d]}).start()
     step(tsem, 3, r5.at[1:4], across).wait_recv()
     r6[core] = (xrows[core] + total(r5, 4)).astype(BF16)
     remote(r6.at[core], r6.at[core], ts.at[4], tr.at[4], mate).start()
-    local[6].wait()
-    step(tsem, 4, r6.at[1 - core], mate).wait_recv()
-    middle = r6[...].astype(F32).reshape(128, 256)
+    swapped = step(tsem, 4, r6.at[1 - core], mate)
     gains = jnp.concatenate(
         [sum(r1b[j, 32:48, :].astype(F32) for j in range(4 * i, 4 * i + 4)) for i in range(2)], axis=1
     )
+    local[6].wait()
+
+    def width(c):
+        return UW + 128 if c == 0 else UW
+
+    def up_half(half, chunks):
+        rows = r6[half].astype(F32)
+        cnormed = (rows * gains[0:1, :]).astype(BF16)
+        mine = pl.ds(half * 8, 8)
+        for c in chunks:
+            if c == 0:
+                msquares = jnp.sum(rows * rows, axis=1, keepdims=True)
+                su[0, mine, :, UW : UW + 128] = jnp.broadcast_to(msquares, (64, 128)).reshape(8, ROWS, 128).astype(BF16)
+            part = jnp.dot(cnormed, wu[:, c * UW : (c + 1) * UW], preferred_element_type=F32)
+            su[c, mine, :, 0:UW] = part.reshape(8, ROWS, UW).astype(BF16)
+            for d in (6, 2, 5, 3, 7, 1, 4, 0):
+                peer = half * 8 + lax.rem(kv + d, 8)
+                copy = remote(
+                    su.at[c, peer, :, 0 : width(c)], ru.at[c, kv, :, 0 : width(c)],
+                    ks.at[7 + c], kr.at[7 + c], {"kv": peer},
+                )
+                if d:
+                    copy.start()
+                else:
+                    pl.when(peer != kv)(copy.start)
+
+    early, late = range(NU // 2), range(NU // 2, NU)
+    up_half(core, early)
+    swapped.wait_recv()
+    up_half(1 - core, early)
+    middle = r6[...].astype(F32).reshape(128, 256)
     cnormed = (middle * gains[0:1, :]).astype(BF16)
-
     up_in, hidden_in = [], []
+    for c in late:
+        part = jnp.dot(cnormed, wu[:, c * UW : (c + 1) * UW], preferred_element_type=F32)
+        su[c, :, :, 0:UW] = part.reshape(KV, ROWS, UW).astype(BF16)
+        for o in PLANE:
+            remote(
+                su.at[c, to[o], :, 0:UW], ru.at[c, kv, :, 0:UW], ks.at[7 + c], kr.at[7 + c], {"kv": to[o]}
+            ).start()
     for c in range(NU):
-        if c == 0:
-            msquares = jnp.sum(middle * middle, axis=1, keepdims=True)
-            su[0, :, :, UW : UW + 128] = jnp.broadcast_to(msquares, (128, 128)).astype(BF16).reshape(KV, ROWS, 128)
-        part = jnp.dot(cnormed, wu[:, c * UW : (c + 1) * UW], preferred_element_type=F32)
-        su[c, :, :, 0:UW] = part.astype(BF16).reshape(KV, ROWS, UW)
-        width = UW + 128 if c == 0 else UW
-        up_in.append(kv_scatter(7 + c, su.at[c, :, :, 0:width], ru.at[c, :, :, 0:width]))
+        ru[c, kv, :, 0 : width(c)] = su[c, kv, :, 0 : width(c)]
+        up_in.append(step(ksem, 7 + c, ru.at[c, 1:KV, :, 0 : width(c)], aside))
     midt[...] = jnp.transpose(middle)
     for c in range(NU):
         up_in[c].wait_recv()
@@ -238,7 +292,7 @@
         hidden_in[c].wait_recv()
         hidden = r7[c].astype(F32).reshape(128, UW).astype(BF16)
         down = down + jnp.dot(hidden, wd[c * UW : (c + 1) * UW, :], preferred_element_type=F32)
-    s8[...] = jnp.transpose(down).astype(BF16).reshape(TP, 32, 128)
+    s8[...] = jnp.transpose(down).reshape(TP, 32, 128).astype(BF16)
     for d in (5, 4, 3, 6, 2, 7, 1):
         remote(s8.at[tpto[d]], r8.at[d], ts.at[5], tr.at[5], {"tp": tpto[d]}).start()
     r8[0] = s8[tp]
@@ -264,16 +318,17 @@
     dma = pltpu.SemaphoreType.DMA
     v = lambda *shape: pltpu.VMEM(shape, BF16)
     f = lambda *shape: pltpu.VMEM(shape, F32)
+    ringed = lambda n: (v(4, 4, ROWS, n), v(4, 4, ROWS, n), v(4, ROWS, n), v(4, ROWS, n))
     scratch = [
         v(256, 512), v(256, 512), v(256, 1024), v(256, 1024), v(1024, 256), v(256, 2048), v(2048, 256), v(2, 1, 32),
         v(32, 128), v(TP, 32, 128), v(48, 128), v(TP, 48, 128),
-        v(KV, ROWS, 512), v(KV, ROWS, 512), v(KV, ROWS, 512), v(KV, ROWS, 512),
-        v(KV, ROWS, 1152), v(KV, ROWS, 1152), v(HPD, KV, ROWS, DV), v(HPD, KV, ROWS, DV),
-        v(HPD, KV, ROWS, DV), v(2, 64, 256), v(64, 256), v(4, 64, 256), v(2, 64, 256),
+        *ringed(512), *ringed(512), *ringed(1152),
+        v(HPD, 4, 4, ROWS, DV), v(HPD, 4, 4, ROWS, DV),
+        v(HPD, 4, ROWS, DV), v(HPD, 4, ROWS, DV), v(HPD, KV, ROWS, DV), v(64, 256), v(64, 256), v(4, 64, 256), v(2, 64, 256),
         v(NU, KV, ROWS, UW + 128), v(NU, KV, ROWS, UW + 128), v(NU, KV, ROWS, UW),
         v(TP, 32, 128), v(TP, 32, 128),
-        f(2, 64, 256), f(512, ROWS), f(512, ROWS), f(ROWS, 1024), f(256, 128),
-        dma((11,)), dma((6,)), dma((6,)), dma((7 + 2 * NU,)), dma((7 + 2 * NU,)),
+        f(2, 64, 256), f(2, 64, 256), f(512, ROWS), f(512, ROWS), f(ROWS, 1024), f(256, 128),
+        dma((11,)), dma((6,)), dma((6,)), dma((12 + 2 * NU,)), dma((12 + 2 * NU,)),
         pltpu.SemaphoreType.REGULAR,
     ]
     out, new_state = pl.pallas_call(

time: 57.4 us -> 56.2 us (0.979)
  Pallas kernels: 56.6 us -> 55.4 us
    pallas_call x1, Pallas kernels: 53.3 us -> 52 us  [per_device(): pl.pallas_call(kernel, name='layer', out_shape=(pltpu.VMEM((32, 128), BF1...]
where the time goes in v4:
time: 56.2 us; the launch traced here: 56 us
  Pallas kernels  55.4 us (99%)
  between operations  0.64 us (1%)
    pallas_call x1, Pallas kernels, per_device(): pl.pallas_call(kernel, name='layer', out_shape=(pltpu.VMEM((32, 128), BF1...  52 us
    pallas_call x1, Pallas kernels, per_device(): pl.pallas_call(writer, name='writer', out_shape=(jax.ShapeDtypeStruct((32...  3.38 us

profile of v4, /device:TPU:1, one launch (start us, length us, event | category | flops | bytes accessed | tf_op | source)
XLA Modules:
  0.0 56.0 jit_solution(9265169643452386290)
XLA Ops:
  0.6 52.0 %layer.1 = (bf16[32,128]{1,0:T(8,128)(2,1)S(1)}, f32[8,2,256,512]{3,2,1,0:T(8,128)S(1)}) custom-call(bf16[32,128]{1,0:T(8,128)(2,1)} %bitcast.4, bf16[1,32]{1,0:T(2,128)(2,1)} %bitcast.5, bf16[1,32]{1,0:T(2,128)(2,1)} %bitcast.6, bf16[256,512]{1,0:T(8,128)(2,1)} %wq_ref.1, bf16[256,512]{1,0:T(8,128)(2,1)} %wk_ref.1, bf16[256,1024]{1,0:T(8,128)(2,1)} %wv_ref.1, ...), custom_call_target="tpu_custom_call" | custom-call | tf_op jit(solution)/shard_map/layer/pallas_call | solution.py:334
  52.7 3.4 %writer.1 = (bf16[32,128]{1,0:T(8,128)(2,1)}, f32[8,2,256,512]{3,2,1,0:T(8,128)}) custom-call(bf16[32,128]{1,0:T(8,128)(2,1)S(1)} %get-tuple-element.6.a_ref, f32[8,2,256,512]{3,2,1,0:T(8,128)S(1)} %get-tuple-element.7.s_ref), custom_call_target="tpu_custom_call" | custom-call | tf_op jit(solution)/shard_map/writer/pallas_call | solution.py:345

commit v5 on v4

--- a/solution.py
+++ b/solution.py
@@ -111,7 +111,7 @@
              (wo_ref, wo), (wu_ref, wu), (wd_ref, wd))
         )
     ]
-    for c in first + local:
+    for c in first + local[:4]:
         c.start()
     for c in first:
         c.wait()
@@ -135,6 +135,8 @@
         remote(s1b, r1b.at[tp], ts.at[1], tr.at[1], {"tp": tpto[d]}).start()
     first_in = step(tsem, 0, r1.at[1:TP], across)
     second_in = step(tsem, 1, r1b.at[1:TP], across)
+    for c in local[4:]:
+        c.start()
     for o in PLANE:
         if o[1] == 0:
             pl.semaphore_signal(plane, inc=1, device_id={"kv": to[o]}, device_id_type=MESH)
@@ -202,9 +204,12 @@
 
     ret[...] = value
     for b in range(ROWS):
-        for h in range(HPD):
-            col = kt[h * DK : (h + 1) * DK, b : b + 1]
-            st_ref[b, h] = rates[h] * st_ref[b, h] + col * ret[b : b + 1, h * DV : (h + 1) * DV]
+
+        @pl.loop(0, HPD)
+        def _(h):
+            col = kt[pl.ds(h * DK, DK), b : b + 1]
+            rate = jnp.where(h == 0, rates[0], rates[1])
+            st_ref[b, h] = rate * st_ref[b, h] + col * ret[b : b + 1, pl.ds(pl.multiple_of(h * DV, DV), DV)]
 
     local[5].wait()
     mixed_in[0].wait_recv()

time: 56.2 us -> 56.2 us (level)
  no operation moved by 1% of the time
where the time goes in v5:
time: 56.2 us; the launch traced here: 56.1 us
  Pallas kernels  55.4 us (99%)
  between operations  0.64 us (1%)
    pallas_call x1, Pallas kernels, per_device(): pl.pallas_call(kernel, name='layer', out_shape=(pltpu.VMEM((32, 128), BF1...  52 us
    pallas_call x1, Pallas kernels, per_device(): pl.pallas_call(writer, name='writer', out_shape=(jax.ShapeDtypeStruct((32...  3.38 us

profile of v5, /device:TPU:1, one launch (start us, length us, event | category | flops | bytes accessed | tf_op | source)
XLA Modules:
  0.0 56.1 jit_solution(7583210858181990241)
XLA Ops:
  0.6 52.0 %layer.1 = (bf16[32,128]{1,0:T(8,128)(2,1)S(1)}, f32[8,2,256,512]{3,2,1,0:T(8,128)S(1)}) custom-call(bf16[32,128]{1,0:T(8,128)(2,1)} %bitcast.4, bf16[1,32]{1,0:T(2,128)(2,1)} %bitcast.5, bf16[1,32]{1,0:T(2,128)(2,1)} %bitcast.6, bf16[256,512]{1,0:T(8,128)(2,1)} %wq_ref.1, bf16[256,512]{1,0:T(8,128)(2,1)} %wk_ref.1, bf16[256,1024]{1,0:T(8,128)(2,1)} %wv_ref.1, ...), custom_call_target="tpu_custom_call" | custom-call | tf_op jit(solution)/shard_map/layer/pallas_call | solution.py:339
  52.7 3.4 %writer.1 = (bf16[32,128]{1,0:T(8,128)(2,1)}, f32[8,2,256,512]{3,2,1,0:T(8,128)}) custom-call(bf16[32,128]{1,0:T(8,128)(2,1)S(1)} %get-tuple-element.6.a_ref, f32[8,2,256,512]{3,2,1,0:T(8,128)S(1)} %get-tuple-element.7.s_ref), custom_call_target="tpu_custom_call" | custom-call | tf_op jit(solution)/shard_map/writer/pallas_call | solution.py:350
